TPU v7x, 32 devices: a whole 2x2x4 slice. The times are simulated.
32 devices in a mesh: sp: 8 (over z, y), tp: 4 (over x, core).
Axes of the slice: x: 2, y: 2, z: 4, core: 2. Of those that a mesh axis runs over, the one named last changes fastest.
Arguments:
- tokens: bfloat16 [2048, 4096], P(('sp', 'tp')), may hold values from -6 to 6, as said below
- query_one: bfloat16 [4096, 1024], P('sp', 'tp'), may hold values from -0.125 to 0.125
- query_two: bfloat16 [4096, 1024], P('sp', 'tp'), may hold values from -0.125 to 0.125
- key_one: bfloat16 [4096, 1024], P('sp', 'tp'), may hold values from -0.125 to 0.125
- key_two: bfloat16 [4096, 1024], P('sp', 'tp'), may hold values from -0.125 to 0.125
- value_weight: bfloat16 [4096, 2048], P('sp', 'tp'), may hold values from -0.09375 to 0.09375
- out_weight: bfloat16 [2048, 4096], P('tp', 'sp'), may hold values from -0.125 to 0.125
- lambdas: float32 [8], P('tp'), may hold values from 0.3 to 0.8
- head_gain: float32 [256], replicated, may hold values from 0.1 to 1.9
Outputs:
- layer_out: bfloat16 [2048, 4096], P(('sp', 'tp'))
Inputs may be any that keep to these rules, and one draw needn't show every extreme that they name: `tokens`: the features' mean changes between 16 equal spans of the sequence.
All inputs are finite; a program needn't handle non-finite values.
Results may differ from a plain program's by a relative error of at most 0.013.
The roundings to bfloat16 on the way count: a program that leaves them out, or rounds other values in their place, can miss the bound.
Values may be sent and summed in bfloat16 or wider, within the bound.
No kernel may reach another device: no remote copies, remote signals or barrier semaphores. Data moves between devices by JAX's collectives and lax.ppermute only.
A program may use at most 128 MiB of HBM per device.

v0:
```python
import functools
import math

import jax
import jax.numpy as jnp
from jax import lax
from jax.experimental import pallas as pl
from jax.experimental.pallas import tpu as pltpu
from jax.sharding import PartitionSpec as P


ROPE_BASE = 500000.0
EPS_NORM = 0.02
MASKED = -1e30
LOG2_E = 1.4426950408889634


SMEM = pl.BlockSpec(memory_space=pltpu.SMEM)
VMEM = pl.BlockSpec(memory_space=pltpu.VMEM)


def room(*shapes):
    held = sum(math.prod(shape) * size for shape, size in shapes)
    return pltpu.CompilerParams(vmem_limit_bytes=min(60 << 20, held + held // 4 + (3 << 20)))


def sweep(low, high, body, carry):
    if high - low <= 4:
        for i in range(low, high):
            carry = body(i, carry)
        return carry
    return lax.fori_loop(low, high, body, carry)


def pack_kernel(dims, place, q1, q2, k1, k2, v, keep, give):
    nc, hp, qk, v_dim = dims
    z, c = place[0], place[3]
    half = v_dim // nc
    for own_core in range(nc):

        @pl.when(c == own_core)
        def _():
            for target, ref in ((own_core, keep), (1 - own_core, give)):
                q, k = ((q1, k1), (q2, k2))[target]
                for b in range(hp):
                    slot = jnp.bitwise_xor(lax.rem(z, hp), b)
                    ref[slot, :, :qk] = q[:, b * qk : (b + 1) * qk]
                    ref[slot, :, qk : 2 * qk] = k[:, b * qk : (b + 1) * qk]
                    low = b * v_dim + target * half
                    ref[slot, :, 2 * qk :] = v[:, low : low + half]


def project_kernel(dims, place, cos_ref, sin_ref, *refs):
    nz, ny, nx, nc, _, depth, qk, windows = dims
    tokens = refs[: nz * nx]
    weights = refs[nz * nx : nz * nx + nz * ny * nc]
    out_ref, acc = refs[nz * nx + nz * ny * nc :]
    z, y = place[0], place[1]
    low, high = windows[0][0], windows[-1][1]
    for r in range(nz):
        for ky in range(ny):
            start = (jnp.bitwise_xor(z, r) * ny + lax.rem(y + ky, ny)) * depth
            cols = pl.ds(pl.multiple_of(start, depth), depth)
            left = jnp.concatenate([t[:, cols] for t in tokens], axis=0)
            for kc in range(nc):
                right = weights[(r * ny + ky) * nc + kc][:, low:high]
                part = jnp.dot(left, right, preferred_element_type=jnp.float32)
                if r or ky:
                    part = part + acc[kc]
                acc[kc] = part
    half = qk // 2
    at = 0
    for first, last, rotated in windows:
        for kc in range(nc):
            value = acc[kc, :, first - low : last - low]
            if rotated:
                a, b = value[:, :half], value[:, half:]
                cos, sin = cos_ref[...], sin_ref[...]
                value = jnp.concatenate([a * cos - b * sin, b * cos + a * sin], axis=1)
            out_ref[:, at : at + last - first] = value.astype(jnp.bfloat16)
            at += last - first


def attend_kernel(dims, place, q_ref, lam_ref, gain_ref, *refs):
    nz, ny, nx, nc, rows, qk, v = dims
    pieces = refs[: ny * nc]
    out_ref, kv_all, s_all = refs[ny * nc :]
    z, y, x, c = (place[i] for i in range(4))
    tile = nx * rows
    block = ny * nc * tile
    half = v // nc
    for ky in range(ny):
        for kc in range(nc):
            piece = pieces[ky * nc + kc]
            slot = lax.rem(y + ky, ny) * nc + lax.rem(c + kc, nc)
            for r in range(nz):
                start = (jnp.bitwise_xor(z, r) * (ny * nc) + slot) * tile
                to = pl.ds(pl.multiple_of(start, tile), tile)
                part = piece[r * tile : (r + 1) * tile, :]
                for m in range(nc):
                    n = (m + kc) % nc
                    kv_all[to, n * qk : (n + 1) * qk] = part[:, m * qk : (m + 1) * qk]
                    kv_all[to, nc * qk + n * half : nc * qk + (n + 1) * half] = part[
                        :, nc * qk + m * half : nc * qk + (m + 1) * half
                    ]

    def offset(index, y_at, c_at):
        x_at = lax.rem(x + index // rows, nx)
        return (y_at * nx + x_at) * nc * rows + c_at * rows + index % rows

    chunk = min(block, 512)
    each = block // chunk
    q_off = offset(lax.broadcasted_iota(jnp.int32, (tile, 1), 0), y, c)
    k_index = lax.broadcasted_iota(jnp.int32, (1, chunk), 1)
    factor = qk ** (-0.5) * LOG2_E

    def key_rows(j):
        return pl.ds(pl.multiple_of(j * chunk, chunk), chunk)

    for t in range(nz):
        q_start = pl.multiple_of(jnp.bitwise_xor(z, t) * tile, tile)
        outs = []
        for m in range(nc):
            q = q_ref[pl.ds(q_start, tile), m * qk : (m + 1) * qk]

            def scores(j, top, masked):
                keys = kv_all[key_rows(j), m * qk : (m + 1) * qk]
                s = lax.dot_general(
                    q, keys, (((1,), (1,)), ((), ())), preferred_element_type=jnp.float32
                )
                if masked:
                    index = k_index + (j - t * each) * chunk
                    slot = index // tile
                    k_off = offset(index % tile, slot // nc, slot % nc)
                    s = jnp.where(k_off <= q_off, s, MASKED)
                s_all[:, key_rows(j)] = s
                return jnp.maximum(top, jnp.max(s, axis=-1, keepdims=True))

            top = jnp.full((tile, 1), MASKED, jnp.float32)
            top = sweep(0, t * each, lambda j, v_: scores(j, v_, False), top)
            top = sweep(t * each, (t + 1) * each, lambda j, v_: scores(j, v_, True), top)

            def gather(j, carry):
                total, acc = carry
                e = jnp.exp2((s_all[:, key_rows(j)] - top) * factor)
                total = total + jnp.sum(e, axis=-1, keepdims=True)
                vals = kv_all[key_rows(j), nc * qk :]
                acc = acc + jnp.dot(
                    e.astype(jnp.bfloat16), vals, preferred_element_type=jnp.float32
                )
                return total, acc

            total, acc = sweep(
                0,
                (t + 1) * each,
                gather,
                (jnp.zeros((tile, 1), jnp.float32), jnp.zeros((tile, v), jnp.float32)),
            )
            outs.append(acc / total)
        one = jnp.where(c == 0, outs[0], outs[1])
        two = jnp.where(c == 0, outs[1], outs[0])
        mixed = one - lam_ref[0] * two
        mixed = jnp.where(
            c == 0, mixed, jnp.concatenate([mixed[:, half:], mixed[:, :half]], axis=1)
        )
        mean = jnp.mean(mixed * mixed, axis=-1, keepdims=True)
        scaled = mixed * lax.rsqrt(mean + EPS_NORM) * gain_ref[...]
        out_ref[t * tile : (t + 1) * tile, :] = scaled.astype(jnp.bfloat16)


def out_kernel(dims, place, *refs):
    nz, ny, nx, nc, hp, v = dims
    chunks = refs[:nz]
    weights = refs[nz : nz + nx * ny * nc]
    out_ref, heads = refs[nz + nx * ny * nc :]
    z, y, c = place[0], place[1], place[3]
    count = chunks[0].shape[0]
    cols = weights[0].shape[1]
    for r in range(nz):
        for kx in range(nx):
            heads[kx, r] = chunks[r][:, kx * v : (kx + 1) * v]
    for ky in range(ny):
        total = jnp.zeros((count, cols), jnp.float32)
        for kx in range(nx):
            for kc in range(nc):
                for b in range(hp):
                    r = jnp.bitwise_xor(lax.rem(c + kc, nc) * hp + b, z)
                    total += jnp.dot(
                        heads[kx, r],
                        weights[(kx * ny + ky) * nc + kc][b * v : (b + 1) * v, :],
                        preferred_element_type=jnp.float32,
                    )
        to = pl.multiple_of(lax.rem(y + ky, ny) * cols, cols)
        out_ref[:, pl.ds(to, cols)] = total.astype(jnp.bfloat16)


def on_device(
    nx,
    tokens,
    query_one,
    query_two,
    key_one,
    key_two,
    value_weight,
    out_weight,
    lambdas,
    head_gain,
):
    sp, tp = lax.axis_size("sp"), lax.axis_size("tp")
    nc = tp // nx
    hp = lambdas.shape[0]
    nz = hp * nc
    ny = sp // nz
    rows = tokens.shape[0]
    span = rows * tp
    depth = query_one.shape[0]
    qk = query_one.shape[1] // hp
    v = value_weight.shape[1] // hp
    half = v // nc
    share = 2 * qk + half
    sp_at, tp_at = lax.axis_index("sp"), lax.axis_index("tp")
    z, y = sp_at // ny, sp_at % ny
    x, c = tp_at // nc, tp_at % nc
    place = jnp.stack([z, y, x, c]).astype(jnp.int32)

    def send(value, where, only=None):
        pairs = []
        for a in range(nz):
            for b in range(ny):
                for d in range(nx):
                    for e in range(nc):
                        if only is not None and a not in only:
                            continue
                        to = where(a, b, d, e)
                        pairs.append(
                            (
                                (a * ny + b) * tp + d * nc + e,
                                (to[0] * ny + to[1]) * tp + to[2] * nc + to[3],
                            )
                        )
        return lax.ppermute(value, ("sp", "tp"), pairs)

    def from_z(value, r):
        return send(value, lambda a, b, d, e: (a ^ r, b, d, e)) if r else value

    def from_y(value, k):
        return send(value, lambda a, b, d, e: (a, (b - k) % ny, d, e)) if k else value

    def from_x(value, k):
        return send(value, lambda a, b, d, e: (a, b, (d - k) % nx, e)) if k else value

    def from_c(value, k):
        return send(value, lambda a, b, d, e: (a, b, d, (e - k) % nc)) if k else value

    if nz == 4:
        mid = (1, 2)
        near = from_z(tokens, 1)
        cross = send(tokens, lambda a, b, d, e: (3 - a, b, d, e), mid)
        out_two = send(cross, lambda a, b, d, e: (a ^ 1, b, d, e), mid)
        mid_two = send(near, lambda a, b, d, e: (3 - a, b, d, e), mid)
        out_three = send(mid_two, lambda a, b, d, e: (a ^ 1, b, d, e), mid)
        in_mid = (z == 1) | (z == 2)
        spans = [
            tokens,
            near,
            jnp.where(in_mid, mid_two, out_two),
            jnp.where(in_mid, cross, out_three),
        ]
    else:
        spans = [from_z(tokens, r) for r in range(nz)]
    token_pieces = [from_x(spans[r], k) for r in range(nz) for k in range(nx)]

    shares = jax.ShapeDtypeStruct((hp, depth, share), jnp.bfloat16)
    keep, give = pl.pallas_call(
        functools.partial(pack_kernel, (nc, hp, qk, v)),
        out_shape=(shares, shares),
        in_specs=[SMEM] + [VMEM] * 5,
        out_specs=(VMEM, VMEM),
        cost_estimate=pl.CostEstimate(
            flops=8 * depth * share * hp, bytes_accessed=8 * depth * share * hp, transcendentals=0
        ),
        name="pack",
    )(place, query_one, query_two, key_one, key_two, value_weight)
    taken = from_c(give, 1)
    weight_pieces = []
    for r in range(nz):
        owner = (z ^ r) // hp
        mine = jnp.where(owner == c, keep[r % hp], taken[r % hp])
        got = from_z(mine, r)
        for ky in range(ny):
            beside = from_y(got, ky)
            for kc in range(nc):
                weight_pieces.append(from_c(beside, kc))

    index = jnp.arange(nz * nx * rows, dtype=jnp.int32)
    at_z = z ^ (index // (nx * rows))
    at_x = (x + (index // rows) % nx) % nx
    positions = (at_z * ny + y) * span + (at_x * nc + c) * rows + index % rows
    turn = qk // 2
    inverse = 1.0 / ROPE_BASE ** (jnp.arange(0, 2 * turn, 2, dtype=jnp.float32) / (2 * turn))
    angles = positions.astype(jnp.float32)[:, None] * inverse[None, :]
    cos_part, sin_part = jnp.cos(angles), jnp.sin(angles)

    total_rows = nz * nx * rows

    def project(windows):
        wide = sum(last - first for first, last, _ in windows)
        return pl.pallas_call(
            functools.partial(project_kernel, (nz, ny, nx, nc, rows, depth, qk, windows)),
            out_shape=jax.ShapeDtypeStruct((total_rows, nc * wide), jnp.bfloat16),
            in_specs=[SMEM] + [VMEM] * (2 + nz * nx + nz * ny * nc),
            out_specs=VMEM,
            scratch_shapes=[pltpu.VMEM((nc, total_rows, wide), jnp.float32)],
            cost_estimate=pl.CostEstimate(
                flops=2 * total_rows * sp * depth * nc * wide,
                bytes_accessed=2 * sp * depth * (total_rows + nc * wide),
                transcendentals=0,
            ),
            compiler_params=room(
                ((total_rows, sp * depth), 2),
                ((sp * depth, nc * share), 2),
                ((total_rows, nc * wide), 6),
            ),
        )(place, cos_part, sin_part, *token_pieces, *weight_pieces)

    kv = project(((qk, 2 * qk, True), (2 * qk, share, False)))
    kv_pieces = []
    for ky in range(ny):
        beside = from_y(kv, ky)
        for kc in range(nc):
            kv_pieces.append(from_c(beside, kc))
    q = project(((0, qk, True),))

    out_pieces = []
    for kx in range(nx):
        over = from_x(out_weight, kx)
        for ky in range(ny):
            beside = from_y(over, ky)
            for kc in range(nc):
                out_pieces.append(from_c(beside, kc))

    lam_all = jnp.stack([from_c(lambdas, k) for k in range(nc)])
    lam = lax.dynamic_slice(lam_all, ((z // hp - c) % nc, z % hp), (1, 1))
    pairs = total_rows * total_rows * ny * nc
    attended = pl.pallas_call(
        functools.partial(attend_kernel, (nz, ny, nx, nc, rows, qk, v)),
        out_shape=jax.ShapeDtypeStruct((total_rows, v), jnp.bfloat16),
        in_specs=[SMEM, VMEM, SMEM, VMEM] + [VMEM] * (ny * nc),
        out_specs=VMEM,
        scratch_shapes=[
            pltpu.VMEM((ny * nc * total_rows, 2 * qk + v), jnp.bfloat16),
            pltpu.VMEM((nx * rows, ny * nc * total_rows), jnp.float32),
        ],
        cost_estimate=pl.CostEstimate(
            flops=4 * pairs * (qk + v),
            bytes_accessed=2 * ny * nc * total_rows * (2 * qk + v),
            transcendentals=2 * pairs,
        ),
        compiler_params=room(
            ((2 * ny * nc * total_rows, 2 * qk + v), 2),
            ((nx * rows, ny * nc * total_rows), 8),
            ((total_rows, v), 4),
        ),
        name="attend",
    )(place, q, lam.reshape(1), head_gain.reshape(1, v), *kv_pieces)

    attended = attended.reshape(nz, nx, rows, v)
    own = jnp.concatenate(
        [from_x(attended[:, (nx - k) % nx], k).reshape(nz * rows, v) for k in range(nx)], axis=1
    )
    chunks = [from_z(own, r) for r in range(nz)]
    cols = ny * out_weight.shape[1]
    result = pl.pallas_call(
        functools.partial(out_kernel, (nz, ny, nx, nc, hp, v)),
        out_shape=jax.ShapeDtypeStruct((nz * rows, cols), jnp.bfloat16),
        in_specs=[SMEM] + [VMEM] * (nz + nx * ny * nc),
        out_specs=VMEM,
        scratch_shapes=[pltpu.VMEM((nx, nz, nz * rows, v), jnp.bfloat16)],
        cost_estimate=pl.CostEstimate(
            flops=2 * nz * rows * nx * nz * v * cols,
            bytes_accessed=2 * nx * nz * v * cols,
            transcendentals=0,
        ),
        compiler_params=room(
            ((nx * nz * v, cols), 2), ((2 * nz * rows, nx * nz * v), 2), ((nz * rows, cols), 6)
        ),
        name="out_project",
    )(place, *chunks, *out_pieces)
    out = jnp.zeros((rows, nz * cols), jnp.bfloat16)
    for r in range(nz):
        mine = lax.dynamic_slice_in_dim(result, (z ^ r) * rows, rows, axis=0)
        out = lax.dynamic_update_slice(out, from_z(mine, r), (0, (z ^ r) * cols))
    return out


def solution(mesh):
    in_specs = (
        P(("sp", "tp"), None),
        P("sp", "tp"),
        P("sp", "tp"),
        P("sp", "tp"),
        P("sp", "tp"),
        P("sp", "tp"),
        P("tp", "sp"),
        P("tp"),
        P(),
    )
    out_specs = P(("sp", "tp"), None)
    nx = 2
    return jax.shard_map(
        functools.partial(on_device, nx),
        mesh=mesh,
        in_specs=in_specs,
        out_specs=out_specs,
        check_vma=False,
    )
```

profile of v0, /device:TPU:0, one launch (start us, length us, event | category | flops | bytes accessed | tf_op | source)
XLA Modules:
  0.0 219.5 jit_solution(10211588405786244719)
XLA Ops:
  0.7 2.8 %pack.1 = (bf16[2,512,384]{2,1,0:T(8,128)(2,1)}, bf16[2,512,384]{2,1,0:T(8,128)(2,1)}) custom-call(s32[4]{0:T(128)} %pad_add_fusion.place, bf16[512,256]{1,0:T(8,128)(2,1)} %q1.1, bf16[512,256]{1,0:T(8,128)(2,1)} %q2.1, bf16[512,256]{1,0:T(8,128)(2,1)} %k1.1, bf16[512,256]{1,0:T(8,128)(2,1)} %k2.1, bf16[512,512]{1,0:T(8,128)(2,1)} %v.1), custom_call_target="tpu_custom_call" | custom-call | flops 3145728 | bytes 3145728 | tf_op jit(solution)/shard_map/pack/pallas_call | solution.py:274
  4.0 2.6 %collective-permute-start.1 = (bf16[64,4096]{1,0:T(8,128)(2,1)S(1)}, bf16[64,4096]{1,0:T(8,128)(2,1)S(1)}, u32[]{:S(2)}, u32[]{:S(2)}) collective-permute-start(bf16[64,4096]{1,0:T(8,128)(2,1)S(1)} %copy-done), channel_id=1, source_target_pairs={{0,8},{1,9},{2,10},{3,11},{4,12},{5,13},{6,14},{7,15},{8,0},{9,1},... | collective-permute-start | bytes 1572872 | tf_op jit(solution)/shard_map/ppermute | solution.py:241
  7.3 11.8 %collective-permute-done.1.refs_2_ = bf16[64,4096]{1,0:T(8,128)(2,1)S(1)} collective-permute-done((bf16[64,4096]{1,0:T(8,128)(2,1)S(1)}, bf16[64,4096]{1,0:T(8,128)(2,1)S(1)}, u32[]{:S(2)}, u32[]{:S(2)}) %collective-permute-start.1) | collective-permute-done | bytes 524320 | tf_op jit(solution)/shard_map/ppermute | solution.py:241
  21.9 1.7 collective-permute-start
  25.3 1.8 collective-permute-start.11
  27.1 10.1 %collective-permute-done.5 = bf16[64,4096]{1,0:T(8,128)(2,1)} collective-permute-done((bf16[64,4096]{1,0:T(8,128)(2,1)S(1)}, bf16[64,4096]{1,0:T(8,128)(2,1)}, u32[]{:S(2)}, u32[]{:S(2)}) %collective-permute-start.5) | collective-permute-done | bytes 524320 | tf_op jit(solution)/shard_map/ppermute | solution.py:241
  38.9 1.6 collective-permute-start.6
  40.5 7.5 %collective-permute-done.2.refs_3_ = bf16[64,4096]{1,0:T(8,128)(2,1)S(1)} collective-permute-done((bf16[64,4096]{1,0:T(8,128)(2,1)S(1)}, bf16[64,4096]{1,0:T(8,128)(2,1)S(1)}, u32[]{:S(2)}, u32[]{:S(2)}) %collective-permute-start.2) | collective-permute-done | bytes 524320 | tf_op jit(solution)/shard_map/ppermute | solution.py:241
  49.3 5.8 %collective-permute-start.17 = (bf16[512,384]{1,0:T(8,128)(2,1)S(1)}, bf16[512,384]{1,0:T(8,128)(2,1)S(1)}, u32[]{:S(2)}, u32[]{:S(2)}) collective-permute-start(bf16[512,384]{1,0:T(8,128)(2,1)S(1)} %get-tuple-element.10), channel_id=1, source_target_pairs={{0,16},{1,17},{2,18},{3,19},{4,20},{5,21},{6,22},{7,23},{8,24},{9,... | collective-permute-start | bytes 1179656 | tf_op jit(solution)/shard_map/ppermute | solution.py:241
  56.3 22.8 %collective-permute-done.17.refs_16_ = bf16[512,384]{1,0:T(8,128)(2,1)S(1)} collective-permute-done((bf16[512,384]{1,0:T(8,128)(2,1)S(1)}, bf16[512,384]{1,0:T(8,128)(2,1)S(1)}, u32[]{:S(2)}, u32[]{:S(2)}) %collective-permute-start.17) | collective-permute-done | bytes 393248 | tf_op jit(solution)/shard_map/ppermute | solution.py:241
  79.1 1.5 collective-permute-start.15
  81.3 1.5 collective-permute-start.23
  82.9 1.6 collective-permute-start.8
  84.5 6.5 %collective-permute-done.15.refs_14_ = bf16[512,384]{1,0:T(8,128)(2,1)S(1)} collective-permute-done((bf16[512,384]{1,0:T(8,128)(2,1)S(1)}, bf16[512,384]{1,0:T(8,128)(2,1)S(1)}, u32[]{:S(2)}, u32[]{:S(2)}) %collective-permute-start.15) | collective-permute-done | bytes 393248 | tf_op jit(solution)/shard_map/ppermute | solution.py:241
  91.6 7.9 %collective-permute-done.19.refs_18_ = bf16[512,384]{1,0:T(8,128)(2,1)S(1)} collective-permute-done((bf16[512,384]{1,0:T(8,128)(2,1)S(1)}, bf16[512,384]{1,0:T(8,128)(2,1)S(1)}, u32[]{:S(2)}, u32[]{:S(2)}) %collective-permute-start.19) | collective-permute-done | bytes 393248 | tf_op jit(solution)/shard_map/ppermute | solution.py:241
  99.5 8.0 %collective-permute-done.23.refs_22_ = bf16[512,384]{1,0:T(8,128)(2,1)S(1)} collective-permute-done((bf16[512,384]{1,0:T(8,128)(2,1)S(1)}, bf16[512,384]{1,0:T(8,128)(2,1)S(1)}, u32[]{:S(2)}, u32[]{:S(2)}) %collective-permute-start.23) | collective-permute-done | bytes 393248 | tf_op jit(solution)/shard_map/ppermute | solution.py:241
  108.5 1.6 collective-permute-start.36
  110.8 3.9 %shard_map.92.refs_0_ = bf16[512,512]{1,0:T(8,128)(2,1)} custom-call(s32[4]{0:T(128)S(1)} %copy-done.39, f32[512,64]{1,0:T(8,128)S(1)} %get-tuple-element.20.cos_ref, f32[512,64]{1,0:T(8,128)S(1)} %get-tuple-element.19.sin_ref, bf16[64,4096]{1,0:T(8,128)(2,1)S(1)} %copy-done, bf16[64,4096]{1,0:T(8,128)(2,1)S(1)} %collective-permute-done.refs_1_, ...), custom_call_target="tpu_custom_call" | custom-call | flops 2147483648 | bytes 8388608 | tf_op jit(solution)/shard_map/pallas_call | solution.py:308
  119.8 3.4 %collective-permute-done.36.refs_8_ = bf16[512,512]{1,0:T(8,128)(2,1)} collective-permute-done((bf16[512,512]{1,0:T(8,128)(2,1)}, bf16[512,512]{1,0:T(8,128)(2,1)}, u32[]{:S(2)}, u32[]{:S(2)}) %collective-permute-start.36) | collective-permute-done | bytes 524320 | tf_op jit(solution)/shard_map/ppermute | solution.py:241
  124.7 8.2 %collective-permute-done.27.refs_2_ = bf16[512,512]{1,0:T(8,128)(2,1)} collective-permute-done((bf16[512,512]{1,0:T(8,128)(2,1)}, bf16[512,512]{1,0:T(8,128)(2,1)}, u32[]{:S(2)}, u32[]{:S(2)}) %collective-permute-start.27) | collective-permute-done | bytes 524320 | tf_op jit(solution)/shard_map/ppermute | solution.py:241
  133.4 1.7 collective-permute-done.25
  154.0 3.1 %shard_map.91.q_ref = bf16[512,256]{1,0:T(8,128)(2,1)S(1)} custom-call(s32[4]{0:T(128)S(1)} %copy-done.39, f32[512,64]{1,0:T(8,128)S(1)} %get-tuple-element.20.cos_ref, f32[512,64]{1,0:T(8,128)S(1)} %get-tuple-element.19.sin_ref, bf16[64,4096]{1,0:T(8,128)(2,1)S(1)} %copy-done, bf16[64,4096]{1,0:T(8,128)(2,1)S(1)} %collective-permute-done.refs_1_, ...), custom_call_target="tpu_custom_call" | custom-call | flops 1073741824 | bytes 6291456 | tf_op jit(solution)/shard_map/pallas_call | solution.py:308
  158.7 5.4 %attend.1 = bf16[512,256]{1,0:T(8,128)(2,1)S(1)} custom-call(s32[4]{0:T(128)S(1)} %copy-done.39, bf16[512,256]{1,0:T(8,128)(2,1)S(1)} %shard_map.91.q_ref, f32[1]{0:T(128)} %bitcast.10.lam_ref, f32[1,256]{1,0:T(1,128)S(1)} %bitcast.26, bf16[512,512]{1,0:T(8,128)(2,1)} %shard_map.92.refs_0_, bf16[512,512]{1,0:T(8,128)(2,1)} %collective-permute-done.26.refs_1_, ...), custom_call_target="tpu_custom_call" | custom-call | flops 1610612736 | bytes 2097152 | tf_op jit(solution)/shard_map/attend/pallas_call | solution.py:345
  164.7 5.0 %collective-permute-done.29 = bf16[4,64,256]{2,1,0:T(8,128)(2,1)S(1)} collective-permute-done((bf16[4,64,256]{2,1,0:T(8,128)(2,1)S(1)}, bf16[4,64,256]{2,1,0:T(8,128)(2,1)S(1)}, u32[]{:S(2)}, u32[]{:S(2)}) %collective-permute-start.29) | collective-permute-done | bytes 131104 | tf_op jit(solution)/shard_map/ppermute | solution.py:241
  169.8 6.6 %collective-permute-start.30 = (bf16[256,512]{1,0:T(8,128)(2,1)S(1)}, bf16[256,512]{1,0:T(8,128)(2,1)S(1)}, u32[]{:S(2)}, u32[]{:S(2)}) collective-permute-start(bf16[256,512]{1,0:T(8,128)(2,1)S(1)} %pad_maximum_fusion.refs_0_), channel_id=1, source_target_pairs={{0,8},{1,9},{2,10},{3,11},{4,12},{5,13},{6,14},{7,15},{8,0},{9,1},... | collective-permute-start | bytes 786440 | tf_op jit(solution)/shard_map/ppermute | solution.py:241
  177.2 2.4 %collective-permute-start.32 = (bf16[256,512]{1,0:T(8,128)(2,1)S(1)}, bf16[256,512]{1,0:T(8,128)(2,1)S(1)}, u32[]{:S(2)}, u32[]{:S(2)}) collective-permute-start(bf16[256,512]{1,0:T(8,128)(2,1)S(1)} %pad_maximum_fusion.refs_0_), channel_id=1, source_target_pairs={{0,24},{1,25},{2,26},{3,27},{4,28},{5,29},{6,30},{7,31},{8,16},{9,... | collective-permute-start | bytes 786440 | tf_op jit(solution)/shard_map/ppermute | solution.py:241
  179.6 5.2 %collective-permute-done.30.refs_1_ = bf16[256,512]{1,0:T(8,128)(2,1)S(1)} collective-permute-done((bf16[256,512]{1,0:T(8,128)(2,1)S(1)}, bf16[256,512]{1,0:T(8,128)(2,1)S(1)}, u32[]{:S(2)}, u32[]{:S(2)}) %collective-permute-start.30) | collective-permute-done | bytes 262176 | tf_op jit(solution)/shard_map/ppermute | solution.py:241
  184.7 13.2 %collective-permute-done.31.refs_2_ = bf16[256,512]{1,0:T(8,128)(2,1)S(1)} collective-permute-done((bf16[256,512]{1,0:T(8,128)(2,1)S(1)}, bf16[256,512]{1,0:T(8,128)(2,1)S(1)}, u32[]{:S(2)}, u32[]{:S(2)}) %collective-permute-start.31) | collective-permute-done | bytes 262176 | tf_op jit(solution)/shard_map/ppermute | solution.py:241
  199.0 2.8 %out_project.1 = bf16[256,1024]{1,0:T(8,128)(2,1)S(1)} custom-call(s32[4]{0:T(128)S(1)} %copy-done.39, bf16[256,512]{1,0:T(8,128)(2,1)S(1)} %pad_maximum_fusion.refs_0_, bf16[256,512]{1,0:T(8,128)(2,1)S(1)} %collective-permute-done.30.refs_1_, bf16[256,512]{1,0:T(8,128)(2,1)S(1)} %collective-permute-done.31.refs_2_, ...), custom_call_target="tpu_custom_call" | custom-call | flops 1073741824 | bytes 4194304 | tf_op jit(solution)/shard_map/out_project/pallas_call | solution.py:373
  201.9 4.8 %collective-permute-start.40 = (bf16[64,1024]{1,0:T(8,128)(2,1)S(1)}, bf16[64,1024]{1,0:T(8,128)(2,1)S(1)}, u32[]{:S(2)}, u32[]{:S(2)}) collective-permute-start(bf16[64,1024]{1,0:T(8,128)(2,1)S(1)} %get-tuple-element.15), channel_id=1, source_target_pairs={{0,8},{1,9},{2,10},{3,11},{4,12},{5,13},{6,14},{7,15},{8,0},{9,1},... | collective-permute-start | bytes 393224 | tf_op jit(solution)/shard_map/ppermute | solution.py:241
  206.7 2.4 %collective-permute-start.42 = (bf16[64,1024]{1,0:T(8,128)(2,1)S(1)}, bf16[64,1024]{1,0:T(8,128)(2,1)S(1)}, u32[]{:S(2)}, u32[]{:S(2)}) collective-permute-start(bf16[64,1024]{1,0:T(8,128)(2,1)S(1)} %get-tuple-element.13), channel_id=1, source_target_pairs={{0,24},{1,25},{2,26},{3,27},{4,28},{5,29},{6,30},{7,31},{8,16},{9,... | collective-permute-start | bytes 393224 | tf_op jit(solution)/shard_map/ppermute | solution.py:241
  210.6 7.4 %collective-permute-done.41 = bf16[64,1024]{1,0:T(8,128)(2,1)S(1)} collective-permute-done((bf16[64,1024]{1,0:T(8,128)(2,1)S(1)}, bf16[64,1024]{1,0:T(8,128)(2,1)S(1)}, u32[]{:S(2)}, u32[]{:S(2)}) %collective-permute-start.41) | collective-permute-done | bytes 131104 | tf_op jit(solution)/shard_map/ppermute | solution.py:241
  (161 shorter events, 46.6 us)
Async XLA Ops:
  3.5 20.5 %collective-permute-start.9 = (bf16[2,512,384]{2,1,0:T(8,128)(2,1)}, bf16[2,512,384]{2,1,0:T(8,128)(2,1)S(1)}, u32[]{:S(2)}, u32[]{:S(2)}) collective-permute-start(bf16[2,512,384]{2,1,0:T(8,128)(2,1)} %get-tuple-element.8), channel_id=1, source_target_pairs={{0,1},{1,0},{2,3},{3,2},{4,5},{5,4},{6,7},{7,6},{8,9},{9,8},{10,11... | collective-permute-start | bytes 2359304 | tf_op jit(solution)/shard_map/ppermute | solution.py:241
  4.0 15.2 %collective-permute-start.1 = (bf16[64,4096]{1,0:T(8,128)(2,1)S(1)}, bf16[64,4096]{1,0:T(8,128)(2,1)S(1)}, u32[]{:S(2)}, u32[]{:S(2)}) collective-permute-start(bf16[64,4096]{1,0:T(8,128)(2,1)S(1)} %copy-done), channel_id=1, source_target_pairs={{0,8},{1,9},{2,10},{3,11},{4,12},{5,13},{6,14},{7,15},{8,0},{9,1},... | collective-permute-start | bytes 1572872 | tf_op jit(solution)/shard_map/ppermute | solution.py:241
  6.6 14.0 %collective-permute-start.4 = (bf16[64,4096]{1,0:T(8,128)(2,1)S(1)}, bf16[64,4096]{1,0:T(8,128)(2,1)S(1)}, u32[]{:S(2)}, u32[]{:S(2)}) collective-permute-start(bf16[64,4096]{1,0:T(8,128)(2,1)S(1)} %copy-done), channel_id=1, source_target_pairs={{8,16},{9,17},{10,18},{11,19},{12,20},{13,21},{14,22},{15,23},{16,... | collective-permute-start | bytes 1572872 | tf_op jit(solution)/shard_map/ppermute | solution.py:241
  20.6 16.5 %collective-permute-start.5 = (bf16[64,4096]{1,0:T(8,128)(2,1)S(1)}, bf16[64,4096]{1,0:T(8,128)(2,1)}, u32[]{:S(2)}, u32[]{:S(2)}) collective-permute-start(bf16[64,4096]{1,0:T(8,128)(2,1)S(1)} %collective-permute-done.4), channel_id=1, source_target_pairs={{8,0},{9,1},{10,2},{11,3},{12,4},{13,5},{14,6},{15,7},{16,24},{17,... | collective-permute-start | bytes 1572872 | tf_op jit(solution)/shard_map/ppermute | solution.py:241
  21.9 17.0 %collective-permute-start = (bf16[64,4096]{1,0:T(8,128)(2,1)S(1)}, bf16[64,4096]{1,0:T(8,128)(2,1)S(1)}, u32[]{:S(2)}, u32[]{:S(2)}) collective-permute-start(bf16[64,4096]{1,0:T(8,128)(2,1)S(1)} %copy-done), channel_id=1, source_target_pairs={{0,2},{1,3},{2,0},{3,1},{4,6},{5,7},{6,4},{7,5},{8,10},{9,11},{10,... | collective-permute-start | bytes 1572872 | tf_op jit(solution)/shard_map/ppermute | solution.py:241
  23.6 24.4 %collective-permute-start.2 = (bf16[64,4096]{1,0:T(8,128)(2,1)S(1)}, bf16[64,4096]{1,0:T(8,128)(2,1)S(1)}, u32[]{:S(2)}, u32[]{:S(2)}) collective-permute-start(bf16[64,4096]{1,0:T(8,128)(2,1)S(1)} %collective-permute-done.1.refs_2_), channel_id=1, source_target_pairs={{0,2},{1,3},{2,0},{3,1},{4,6},{5,7},{6,4},{7,5},{8,10},{9,11},{10,... | collective-permute-start | bytes 1572872 | tf_op jit(solution)/shard_map/ppermute | solution.py:241
  25.3 24.0 %collective-permute-start.10 = (bf16[512,384]{1,0:T(8,128)(2,1)S(1)}, bf16[512,384]{1,0:T(8,128)(2,1)S(1)}, u32[]{:S(2)}, u32[]{:S(2)}) collective-permute-start(bf16[512,384]{1,0:T(8,128)(2,1)S(1)} %get-tuple-element.12.refs_8_), channel_id=1, source_target_pairs={{0,1},{1,0},{2,3},{3,2},{4,5},{5,4},{6,7},{7,6},{8,9},{9,8},{10,11... | collective-permute-start | bytes 1179656 | tf_op jit(solution)/shard_map/ppermute | solution.py:241
  25.3 29.7 %collective-permute-start.11 = (bf16[512,384]{1,0:T(8,128)(2,1)S(1)}, bf16[512,384]{1,0:T(8,128)(2,1)S(1)}, u32[]{:S(2)}, u32[]{:S(2)}) collective-permute-start(bf16[512,384]{1,0:T(8,128)(2,1)S(1)} %get-tuple-element.12.refs_8_), channel_id=1, source_target_pairs={{0,4},{1,5},{2,6},{3,7},{4,0},{5,1},{6,2},{7,3},{8,12},{9,13},{10,... | collective-permute-start | bytes 1179656 | tf_op jit(solution)/shard_map/ppermute | solution.py:241
  37.2 19.1 %collective-permute-start.13 = (bf16[512,384]{1,0:T(8,128)(2,1)S(1)}, bf16[512,384]{1,0:T(8,128)(2,1)S(1)}, u32[]{:S(2)}, u32[]{:S(2)}) collective-permute-start(bf16[512,384]{1,0:T(8,128)(2,1)S(1)} %get-tuple-element.11), channel_id=1, source_target_pairs={{0,8},{1,9},{2,10},{3,11},{4,12},{5,13},{6,14},{7,15},{8,0},{9,1},... | collective-permute-start | bytes 1179656 | tf_op jit(solution)/shard_map/ppermute | solution.py:241
  38.9 41.7 %collective-permute-start.6 = (bf16[64,4096]{1,0:T(8,128)(2,1)S(1)}, bf16[64,4096]{1,0:T(8,128)(2,1)S(1)}, u32[]{:S(2)}, u32[]{:S(2)}) collective-permute-start(bf16[64,4096]{1,0:T(8,128)(2,1)S(1)} %broadcast_select_fusion.1.refs_4_), channel_id=1, source_target_pairs={{0,2},{1,3},{2,0},{3,1},{4,6},{5,7},{6,4},{7,5},{8,10},{9,11},{10,... | collective-permute-start | bytes 1572872 | tf_op jit(solution)/shard_map/ppermute | solution.py:241
  48.0 32.8 %collective-permute-start.7 = (bf16[64,4096]{1,0:T(8,128)(2,1)}, bf16[64,4096]{1,0:T(8,128)(2,1)S(1)}, u32[]{:S(2)}, u32[]{:S(2)}) collective-permute-start(bf16[64,4096]{1,0:T(8,128)(2,1)} %collective-permute-done.3), channel_id=1, source_target_pairs={{8,0},{9,1},{10,2},{11,3},{12,4},{13,5},{14,6},{15,7},{16,24},{17,... | collective-permute-start | bytes 1572872 | tf_op jit(solution)/shard_map/ppermute | solution.py:241
  49.3 29.8 %collective-permute-start.17 = (bf16[512,384]{1,0:T(8,128)(2,1)S(1)}, bf16[512,384]{1,0:T(8,128)(2,1)S(1)}, u32[]{:S(2)}, u32[]{:S(2)}) collective-permute-start(bf16[512,384]{1,0:T(8,128)(2,1)S(1)} %get-tuple-element.10), channel_id=1, source_target_pairs={{0,16},{1,17},{2,18},{3,19},{4,20},{5,21},{6,22},{7,23},{8,24},{9,... | collective-permute-start | bytes 1179656 | tf_op jit(solution)/shard_map/ppermute | solution.py:241
  55.1 24.0 %collective-permute-start.21 = (bf16[512,384]{1,0:T(8,128)(2,1)S(1)}, bf16[512,384]{1,0:T(8,128)(2,1)S(1)}, u32[]{:S(2)}, u32[]{:S(2)}) collective-permute-start(bf16[512,384]{1,0:T(8,128)(2,1)S(1)} %get-tuple-element.9), channel_id=1, source_target_pairs={{0,24},{1,25},{2,26},{3,27},{4,28},{5,29},{6,30},{7,31},{8,16},{9,... | collective-permute-start | bytes 1179656 | tf_op jit(solution)/shard_map/ppermute | solution.py:241
  56.3 25.0 %collective-permute-start.12 = (bf16[512,384]{1,0:T(8,128)(2,1)S(1)}, bf16[512,384]{1,0:T(8,128)(2,1)S(1)}, u32[]{:S(2)}, u32[]{:S(2)}) collective-permute-start(bf16[512,384]{1,0:T(8,128)(2,1)S(1)} %collective-permute-done.11.refs_10_), channel_id=1, source_target_pairs={{0,1},{1,0},{2,3},{3,2},{4,5},{5,4},{6,7},{7,6},{8,9},{9,8},{10,11... | collective-permute-start | bytes 1179656 | tf_op jit(solution)/shard_map/ppermute | solution.py:241
  80.8 18.7 %collective-permute-start.19 = (bf16[512,384]{1,0:T(8,128)(2,1)S(1)}, bf16[512,384]{1,0:T(8,128)(2,1)S(1)}, u32[]{:S(2)}, u32[]{:S(2)}) collective-permute-start(bf16[512,384]{1,0:T(8,128)(2,1)S(1)} %collective-permute-done.17.refs_16_), channel_id=1, source_target_pairs={{0,4},{1,5},{2,6},{3,7},{4,0},{5,1},{6,2},{7,3},{8,12},{9,13},{10,... | collective-permute-start | bytes 1179656 | tf_op jit(solution)/shard_map/ppermute | solution.py:241
  81.3 26.1 %collective-permute-start.23 = (bf16[512,384]{1,0:T(8,128)(2,1)S(1)}, bf16[512,384]{1,0:T(8,128)(2,1)S(1)}, u32[]{:S(2)}, u32[]{:S(2)}) collective-permute-start(bf16[512,384]{1,0:T(8,128)(2,1)S(1)} %collective-permute-done.21.refs_20_), channel_id=1, source_target_pairs={{0,4},{1,5},{2,6},{3,7},{4,0},{5,1},{6,2},{7,3},{8,12},{9,13},{10,... | collective-permute-start | bytes 1179656 | tf_op jit(solution)/shard_map/ppermute | solution.py:241
  82.9 27.1 %collective-permute-start.8 = (bf16[64,4096]{1,0:T(8,128)(2,1)S(1)}, bf16[64,4096]{1,0:T(8,128)(2,1)S(1)}, u32[]{:S(2)}, u32[]{:S(2)}) collective-permute-start(bf16[64,4096]{1,0:T(8,128)(2,1)S(1)} %broadcast_select_fusion.refs_6_), channel_id=1, source_target_pairs={{0,2},{1,3},{2,0},{3,1},{4,6},{5,7},{6,4},{7,5},{8,10},{9,11},{10,... | collective-permute-start | bytes 1572872 | tf_op jit(solution)/shard_map/ppermute | solution.py:241
  91.1 17.4 %collective-permute-start.22 = (bf16[512,384]{1,0:T(8,128)(2,1)S(1)}, bf16[512,384]{1,0:T(8,128)(2,1)S(1)}, u32[]{:S(2)}, u32[]{:S(2)}) collective-permute-start(bf16[512,384]{1,0:T(8,128)(2,1)S(1)} %collective-permute-done.21.refs_20_), channel_id=1, source_target_pairs={{0,1},{1,0},{2,3},{3,2},{4,5},{5,4},{6,7},{7,6},{8,9},{9,8},{10,11... | collective-permute-start | bytes 1179656 | tf_op jit(solution)/shard_map/ppermute | solution.py:241
  91.1 19.0 %collective-permute-start.16 = (bf16[512,384]{1,0:T(8,128)(2,1)S(1)}, bf16[512,384]{1,0:T(8,128)(2,1)S(1)}, u32[]{:S(2)}, u32[]{:S(2)}) collective-permute-start(bf16[512,384]{1,0:T(8,128)(2,1)S(1)} %collective-permute-done.15.refs_14_), channel_id=1, source_target_pairs={{0,1},{1,0},{2,3},{3,2},{4,5},{5,4},{6,7},{7,6},{8,9},{9,8},{10,11... | collective-permute-start | bytes 1179656 | tf_op jit(solution)/shard_map/ppermute | solution.py:241
  108.5 14.7 %collective-permute-start.36 = (bf16[512,512]{1,0:T(8,128)(2,1)}, bf16[512,512]{1,0:T(8,128)(2,1)}, u32[]{:S(2)}, u32[]{:S(2)}) collective-permute-start(bf16[512,512]{1,0:T(8,128)(2,1)} %refs_4_.1), channel_id=1, source_target_pairs={{0,2},{1,3},{2,0},{3,1},{4,6},{5,7},{6,4},{7,5},{8,10},{9,11},{10,... | collective-permute-start | bytes 1572872 | tf_op jit(solution)/shard_map/ppermute | solution.py:241
  117.8 15.1 %collective-permute-start.27 = (bf16[512,512]{1,0:T(8,128)(2,1)}, bf16[512,512]{1,0:T(8,128)(2,1)}, u32[]{:S(2)}, u32[]{:S(2)}) collective-permute-start(bf16[512,512]{1,0:T(8,128)(2,1)} %shard_map.92.refs_0_), channel_id=1, source_target_pairs={{0,4},{1,5},{2,6},{3,7},{4,0},{5,1},{6,2},{7,3},{8,12},{9,13},{10,... | collective-permute-start | bytes 1572872 | tf_op jit(solution)/shard_map/ppermute | solution.py:241
  119.3 37.8 %collective-permute-start.34 = (bf16[512,512]{1,0:T(8,128)(2,1)}, bf16[512,512]{1,0:T(8,128)(2,1)}, u32[]{:S(2)}, u32[]{:S(2)}) collective-permute-start(bf16[512,512]{1,0:T(8,128)(2,1)} %refs_4_.1), channel_id=1, source_target_pairs={{0,4},{1,5},{2,6},{3,7},{4,0},{5,1},{6,2},{7,3},{8,12},{9,13},{10,... | collective-permute-start | bytes 1572872 | tf_op jit(solution)/shard_map/ppermute | solution.py:241
  123.2 34.3 %collective-permute-start.38 = (bf16[512,512]{1,0:T(8,128)(2,1)}, bf16[512,512]{1,0:T(8,128)(2,1)}, u32[]{:S(2)}, u32[]{:S(2)}) collective-permute-start(bf16[512,512]{1,0:T(8,128)(2,1)} %collective-permute-done.36.refs_8_), channel_id=1, source_target_pairs={{0,4},{1,5},{2,6},{3,7},{4,0},{5,1},{6,2},{7,3},{8,12},{9,13},{10,... | collective-permute-start | bytes 1572872 | tf_op jit(solution)/shard_map/ppermute | solution.py:241
  124.7 33.0 %collective-permute-start.26 = (bf16[512,512]{1,0:T(8,128)(2,1)}, bf16[512,512]{1,0:T(8,128)(2,1)}, u32[]{:S(2)}, u32[]{:S(2)}) collective-permute-start(bf16[512,512]{1,0:T(8,128)(2,1)} %shard_map.92.refs_0_), channel_id=1, source_target_pairs={{0,1},{1,0},{2,3},{3,2},{4,5},{5,4},{6,7},{7,6},{8,9},{9,8},{10,11... | collective-permute-start | bytes 1572872 | tf_op jit(solution)/shard_map/ppermute | solution.py:241
  132.9 25.1 %collective-permute-start.28 = (bf16[512,512]{1,0:T(8,128)(2,1)}, bf16[512,512]{1,0:T(8,128)(2,1)}, u32[]{:S(2)}, u32[]{:S(2)}) collective-permute-start(bf16[512,512]{1,0:T(8,128)(2,1)} %collective-permute-done.27.refs_2_), channel_id=1, source_target_pairs={{0,1},{1,0},{2,3},{3,2},{4,5},{5,4},{6,7},{7,6},{8,9},{9,8},{10,11... | collective-permute-start | bytes 1572872 | tf_op jit(solution)/shard_map/ppermute | solution.py:241
  135.2 41.2 %collective-permute-start.33 = (bf16[512,512]{1,0:T(8,128)(2,1)}, bf16[512,512]{1,0:T(8,128)(2,1)S(1)}, u32[]{:S(2)}, u32[]{:S(2)}) collective-permute-start(bf16[512,512]{1,0:T(8,128)(2,1)} %refs_4_.1), channel_id=1, source_target_pairs={{0,1},{1,0},{2,3},{3,2},{4,5},{5,4},{6,7},{7,6},{8,9},{9,8},{10,11... | collective-permute-start | bytes 1572872 | tf_op jit(solution)/shard_map/ppermute | solution.py:241
  157.1 22.5 %collective-permute-start.37 = (bf16[512,512]{1,0:T(8,128)(2,1)}, bf16[512,512]{1,0:T(8,128)(2,1)S(1)}, u32[]{:S(2)}, u32[]{:S(2)}) collective-permute-start(bf16[512,512]{1,0:T(8,128)(2,1)} %collective-permute-done.36.refs_8_), channel_id=1, source_target_pairs={{0,1},{1,0},{2,3},{3,2},{4,5},{5,4},{6,7},{7,6},{8,9},{9,8},{10,11... | collective-permute-start | bytes 1572872 | tf_op jit(solution)/shard_map/ppermute | solution.py:241
  157.5 19.6 %collective-permute-start.35 = (bf16[512,512]{1,0:T(8,128)(2,1)}, bf16[512,512]{1,0:T(8,128)(2,1)S(1)}, u32[]{:S(2)}, u32[]{:S(2)}) collective-permute-start(bf16[512,512]{1,0:T(8,128)(2,1)} %collective-permute-done.34.refs_6_), channel_id=1, source_target_pairs={{0,1},{1,0},{2,3},{3,2},{4,5},{5,4},{6,7},{7,6},{8,9},{9,8},{10,11... | collective-permute-start | bytes 1572872 | tf_op jit(solution)/shard_map/ppermute | solution.py:241
  157.7 21.9 %collective-permute-start.39 = (bf16[512,512]{1,0:T(8,128)(2,1)}, bf16[512,512]{1,0:T(8,128)(2,1)S(1)}, u32[]{:S(2)}, u32[]{:S(2)}) collective-permute-start(bf16[512,512]{1,0:T(8,128)(2,1)} %collective-permute-done.38.refs_10_), channel_id=1, source_target_pairs={{0,1},{1,0},{2,3},{3,2},{4,5},{5,4},{6,7},{7,6},{8,9},{9,8},{10,11... | collective-permute-start | bytes 1572872 | tf_op jit(solution)/shard_map/ppermute | solution.py:241
  169.8 15.0 %collective-permute-start.30 = (bf16[256,512]{1,0:T(8,128)(2,1)S(1)}, bf16[256,512]{1,0:T(8,128)(2,1)S(1)}, u32[]{:S(2)}, u32[]{:S(2)}) collective-permute-start(bf16[256,512]{1,0:T(8,128)(2,1)S(1)} %pad_maximum_fusion.refs_0_), channel_id=1, source_target_pairs={{0,8},{1,9},{2,10},{3,11},{4,12},{5,13},{6,14},{7,15},{8,0},{9,1},... | collective-permute-start | bytes 786440 | tf_op jit(solution)/shard_map/ppermute | solution.py:241
  177.2 20.8 %collective-permute-start.31 = (bf16[256,512]{1,0:T(8,128)(2,1)S(1)}, bf16[256,512]{1,0:T(8,128)(2,1)S(1)}, u32[]{:S(2)}, u32[]{:S(2)}) collective-permute-start(bf16[256,512]{1,0:T(8,128)(2,1)S(1)} %pad_maximum_fusion.refs_0_), channel_id=1, source_target_pairs={{0,16},{1,17},{2,18},{3,19},{4,20},{5,21},{6,22},{7,23},{8,24},{9,... | collective-permute-start | bytes 786440 | tf_op jit(solution)/shard_map/ppermute | solution.py:241
  177.2 20.8 %collective-permute-start.32 = (bf16[256,512]{1,0:T(8,128)(2,1)S(1)}, bf16[256,512]{1,0:T(8,128)(2,1)S(1)}, u32[]{:S(2)}, u32[]{:S(2)}) collective-permute-start(bf16[256,512]{1,0:T(8,128)(2,1)S(1)} %pad_maximum_fusion.refs_0_), channel_id=1, source_target_pairs={{0,24},{1,25},{2,26},{3,27},{4,28},{5,29},{6,30},{7,31},{8,16},{9,... | collective-permute-start | bytes 786440 | tf_op jit(solution)/shard_map/ppermute | solution.py:241
  (54 other events, 469.8 us)
where the time goes:
time: 221 us; the launch traced here: 220 us
  waiting for transfers between devices  120 us (54%)
  starting transfers between devices  50.3 us (23%)
  local copies, waits for them, and re-layouts  26.4 us (12%)
  Pallas kernels  18 us (8%)
  other arithmetic  4.13 us (2%)
    ppermute x43, waiting for transfers between devices, send(): return lax.ppermute(value, ('sp', 'tp'), pairs)  120 us
    ppermute x43, starting transfers between devices, send(): return lax.ppermute(value, ('sp', 'tp'), pairs)  50.3 us
    unnamed x86, local copies, waits for them, and re-layouts  25 us
    pallas_call x2, Pallas kernels, project(): pl.pallas_call(functools.partial(project_kernel, (nz, ny, nx, nc, rows, d...  7.02 us
    pallas_call x1, Pallas kernels, on_device(): pl.pallas_call(functools.partial(attend_kernel, (nz, ny, nx, nc, rows, qk...  5.35 us
  transfers between devices with their start and end apart: 43, of which 15 were waited for; matrix products, arithmetic and copies ran while one was open for 2% of the time, Pallas kernels for 6%

commit v1 on v0

--- a/solution.py
+++ b/solution.py
@@ -32,29 +32,29 @@
     return lax.fori_loop(low, high, body, carry)
 
 
-def pack_kernel(dims, place, q1, q2, k1, k2, v, keep, give):
-    nc, hp, qk, v_dim = dims
+def pack_kernel(dims, place, q1, q2, k1, k2, v, keep, give, keep_q, give_q):
+    _, nc, _, hp, qk, v_dim = dims
     z, c = place[0], place[3]
     half = v_dim // nc
     for own_core in range(nc):
 
         @pl.when(c == own_core)
         def _():
-            for target, ref in ((own_core, keep), (1 - own_core, give)):
+            for target, ref, q_ref in ((own_core, keep, keep_q), (1 - own_core, give, give_q)):
                 q, k = ((q1, k1), (q2, k2))[target]
                 for b in range(hp):
                     slot = jnp.bitwise_xor(lax.rem(z, hp), b)
-                    ref[slot, :, :qk] = q[:, b * qk : (b + 1) * qk]
-                    ref[slot, :, qk : 2 * qk] = k[:, b * qk : (b + 1) * qk]
+                    q_ref[slot] = q[:, b * qk : (b + 1) * qk]
+                    ref[slot, :, :qk] = k[:, b * qk : (b + 1) * qk]
                     low = b * v_dim + target * half
-                    ref[slot, :, 2 * qk :] = v[:, low : low + half]
+                    ref[slot, :, qk:] = v[:, low : low + half]
 
 
 def project_kernel(dims, place, cos_ref, sin_ref, *refs):
-    nz, ny, nx, nc, _, depth, qk, windows = dims
+    nz, ny, nx, nc, _, depth, qk, windows, stacked = dims
     tokens = refs[: nz * nx]
-    weights = refs[nz * nx : nz * nx + nz * ny * nc]
-    out_ref, acc = refs[nz * nx + nz * ny * nc :]
+    weights = refs[nz * nx : -2]
+    out_ref, acc = refs[-2:]
     z, y = place[0], place[1]
     low, high = windows[0][0], windows[-1][1]
     for r in range(nz):
@@ -63,7 +63,10 @@
             cols = pl.ds(pl.multiple_of(start, depth), depth)
             left = jnp.concatenate([t[:, cols] for t in tokens], axis=0)
             for kc in range(nc):
-                right = weights[(r * ny + ky) * nc + kc][:, low:high]
+                if stacked:
+                    right = weights[ky * nc + kc][r * depth : (r + 1) * depth, low:high]
+                else:
+                    right = weights[(r * ny + ky) * nc + kc][:, low:high]
                 part = jnp.dot(left, right, preferred_element_type=jnp.float32)
                 if r or ky:
                     part = part + acc[kc]
@@ -81,7 +84,7 @@
             at += last - first
 
 
-def attend_kernel(dims, place, q_ref, lam_ref, gain_ref, *refs):
+def attend_kernel(dims, place, q_ref, lam_own, lam_other, gain_ref, *refs):
     nz, ny, nx, nc, rows, qk, v = dims
     pieces = refs[: ny * nc]
     out_ref, kv_all, s_all = refs[ny * nc :]
@@ -89,6 +92,9 @@
     tile = nx * rows
     block = ny * nc * tile
     half = v // nc
+    hp = nz // nc
+    lam_at = lax.rem(z, hp)
+    lam = jnp.where(z // hp == c, lam_own[lam_at], lam_other[lam_at])
     for ky in range(ny):
         for kc in range(nc):
             piece = pieces[ky * nc + kc]
@@ -159,7 +165,7 @@
             outs.append(acc / total)
         one = jnp.where(c == 0, outs[0], outs[1])
         two = jnp.where(c == 0, outs[1], outs[0])
-        mixed = one - lam_ref[0] * two
+        mixed = one - lam * two
         mixed = jnp.where(
             c == 0, mixed, jnp.concatenate([mixed[:, half:], mixed[:, :half]], axis=1)
         )
@@ -170,15 +176,15 @@
 
 def out_kernel(dims, place, *refs):
     nz, ny, nx, nc, hp, v = dims
-    chunks = refs[:nz]
-    weights = refs[nz : nz + nx * ny * nc]
-    out_ref, heads = refs[nz + nx * ny * nc :]
+    chunks = refs[: nx * nz]
+    weights = refs[nx * nz : nx * nz + nx * ny * nc]
+    out_ref, heads = refs[nx * nz + nx * ny * nc :]
     z, y, c = place[0], place[1], place[3]
     count = chunks[0].shape[0]
     cols = weights[0].shape[1]
-    for r in range(nz):
-        for kx in range(nx):
-            heads[kx, r] = chunks[r][:, kx * v : (kx + 1) * v]
+    for kx in range(nx):
+        for r in range(nz):
+            heads[kx, r] = chunks[kx * nz + r][...]
     for ky in range(ny):
         total = jnp.zeros((count, cols), jnp.float32)
         for kx in range(nx):
@@ -217,7 +223,7 @@
     qk = query_one.shape[1] // hp
     v = value_weight.shape[1] // hp
     half = v // nc
-    share = 2 * qk + half
+    share = qk + half
     sp_at, tp_at = lax.axis_index("sp"), lax.axis_index("tp")
     z, y = sp_at // ny, sp_at % ny
     x, c = tp_at // nc, tp_at % nc
@@ -271,26 +277,35 @@
     token_pieces = [from_x(spans[r], k) for r in range(nz) for k in range(nx)]
 
     shares = jax.ShapeDtypeStruct((hp, depth, share), jnp.bfloat16)
-    keep, give = pl.pallas_call(
-        functools.partial(pack_kernel, (nc, hp, qk, v)),
-        out_shape=(shares, shares),
+    q_shares = jax.ShapeDtypeStruct((hp, depth, qk), jnp.bfloat16)
+    keep, give, keep_q, give_q = pl.pallas_call(
+        functools.partial(pack_kernel, (nx, nc, ny, hp, qk, v)),
+        out_shape=(shares, shares, q_shares, q_shares),
         in_specs=[SMEM] + [VMEM] * 5,
-        out_specs=(VMEM, VMEM),
+        out_specs=(VMEM,) * 4,
         cost_estimate=pl.CostEstimate(
             flops=8 * depth * share * hp, bytes_accessed=8 * depth * share * hp, transcendentals=0
         ),
         name="pack",
     )(place, query_one, query_two, key_one, key_two, value_weight)
-    taken = from_c(give, 1)
-    weight_pieces = []
+    taken, taken_q = from_c(give, 1), from_c(give_q, 1)
+    weight_pieces, q_rows = [], []
     for r in range(nz):
-        owner = (z ^ r) // hp
-        mine = jnp.where(owner == c, keep[r % hp], taken[r % hp])
-        got = from_z(mine, r)
+        own_core = (z ^ r) // hp == c
+        got = from_z(jnp.where(own_core, keep[r % hp], taken[r % hp]), r)
         for ky in range(ny):
             beside = from_y(got, ky)
             for kc in range(nc):
                 weight_pieces.append(from_c(beside, kc))
+    for r in range(nz):
+        own_core = (z ^ r) // hp == c
+        q_rows.append(from_z(jnp.where(own_core, keep_q[r % hp], taken_q[r % hp]), r))
+    q_rows = jnp.concatenate(q_rows, axis=0)
+    q_pieces = []
+    for ky in range(ny):
+        beside = from_y(q_rows, ky)
+        for kc in range(nc):
+            q_pieces.append(from_c(beside, kc))
 
     index = jnp.arange(nz * nx * rows, dtype=jnp.int32)
     at_z = z ^ (index // (nx * rows))
@@ -303,12 +318,13 @@
 
     total_rows = nz * nx * rows
 
-    def project(windows):
+    def project(windows, weights):
         wide = sum(last - first for first, last, _ in windows)
+        stacked = len(weights) < nz * ny * nc
         return pl.pallas_call(
-            functools.partial(project_kernel, (nz, ny, nx, nc, rows, depth, qk, windows)),
+            functools.partial(project_kernel, (nz, ny, nx, nc, rows, depth, qk, windows, stacked)),
             out_shape=jax.ShapeDtypeStruct((total_rows, nc * wide), jnp.bfloat16),
-            in_specs=[SMEM] + [VMEM] * (2 + nz * nx + nz * ny * nc),
+            in_specs=[SMEM] + [VMEM] * (2 + nz * nx + len(weights)),
             out_specs=VMEM,
             scratch_shapes=[pltpu.VMEM((nc, total_rows, wide), jnp.float32)],
             cost_estimate=pl.CostEstimate(
@@ -318,18 +334,18 @@
             ),
             compiler_params=room(
                 ((total_rows, sp * depth), 2),
-                ((sp * depth, nc * share), 2),
+                ((sp * depth, nc * (share + qk)), 2),
                 ((total_rows, nc * wide), 6),
             ),
-        )(place, cos_part, sin_part, *token_pieces, *weight_pieces)
-
-    kv = project(((qk, 2 * qk, True), (2 * qk, share, False)))
+        )(place, cos_part, sin_part, *token_pieces, *weights)
+
+    kv = project(((0, qk, True), (qk, share, False)), weight_pieces)
     kv_pieces = []
     for ky in range(ny):
         beside = from_y(kv, ky)
         for kc in range(nc):
             kv_pieces.append(from_c(beside, kc))
-    q = project(((0, qk, True),))
+    q = project(((0, qk, True),), q_pieces)
 
     out_pieces = []
     for kx in range(nx):
@@ -339,13 +355,12 @@
             for kc in range(nc):
                 out_pieces.append(from_c(beside, kc))
 
-    lam_all = jnp.stack([from_c(lambdas, k) for k in range(nc)])
-    lam = lax.dynamic_slice(lam_all, ((z // hp - c) % nc, z % hp), (1, 1))
+    lam_other = from_c(lambdas, 1)
     pairs = total_rows * total_rows * ny * nc
     attended = pl.pallas_call(
         functools.partial(attend_kernel, (nz, ny, nx, nc, rows, qk, v)),
         out_shape=jax.ShapeDtypeStruct((total_rows, v), jnp.bfloat16),
-        in_specs=[SMEM, VMEM, SMEM, VMEM] + [VMEM] * (ny * nc),
+        in_specs=[SMEM, VMEM, SMEM, SMEM, VMEM] + [VMEM] * (ny * nc),
         out_specs=VMEM,
         scratch_shapes=[
             pltpu.VMEM((ny * nc * total_rows, 2 * qk + v), jnp.bfloat16),
@@ -362,18 +377,23 @@
             ((total_rows, v), 4),
         ),
         name="attend",
-    )(place, q, lam.reshape(1), head_gain.reshape(1, v), *kv_pieces)
+    )(place, q, lambdas, lam_other, head_gain.reshape(1, v), *kv_pieces)
 
     attended = attended.reshape(nz, nx, rows, v)
-    own = jnp.concatenate(
-        [from_x(attended[:, (nx - k) % nx], k).reshape(nz * rows, v) for k in range(nx)], axis=1
-    )
-    chunks = [from_z(own, r) for r in range(nz)]
+    chunks = []
+    for k in range(nx):
+        mine = attended[:, k].reshape(nz * rows, v)
+        for r in range(nz):
+            chunks.append(
+                send(mine, lambda a, b, d, e, k=k, r=r: (a ^ r, b, (d + k) % nx, e))
+                if k or r
+                else mine
+            )
     cols = ny * out_weight.shape[1]
     result = pl.pallas_call(
         functools.partial(out_kernel, (nz, ny, nx, nc, hp, v)),
         out_shape=jax.ShapeDtypeStruct((nz * rows, cols), jnp.bfloat16),
-        in_specs=[SMEM] + [VMEM] * (nz + nx * ny * nc),
+        in_specs=[SMEM] + [VMEM] * (nx * nz + nx * ny * nc),
         out_specs=VMEM,
         scratch_shapes=[pltpu.VMEM((nx, nz, nz * rows, v), jnp.bfloat16)],
         cost_estimate=pl.CostEstimate(

time: 221 us -> 210 us (0.950)
  local copies, waits for them, and re-layouts: 26.4 us -> 11 us
  starting transfers between devices: 50.3 us -> 57.9 us
  Pallas kernels: 18 us -> 14.7 us
    unnamed x86 -> x58, local copies, waits for them, and re-layouts: 25 us -> 10.2 us
    ppermute x43 -> x53, starting transfers between devices: 50.3 us -> 57.9 us  [send(): return lax.ppermute(value, ('sp', 'tp'), pairs)]
    ppermute x43 -> x53, waiting for transfers between devices: 120 us -> 119 us  [send(): return lax.ppermute(value, ('sp', 'tp'), pairs)]
  transfers between devices with their start and end apart: 43 -> 53, of which waited for: 15 -> 19; matrix products, arithmetic and copies ran while one was open for 2% -> 2% of each run, Pallas kernels for 6% -> 5%
where the time goes in v1:
time: 210 us; the launch traced here: 209 us
  waiting for transfers between devices  119 us (57%)
  starting transfers between devices  57.9 us (28%)
  Pallas kernels  14.7 us (7%)
  local copies, waits for them, and re-layouts  11 us (5%)
  other arithmetic  5.81 us (3%)
    ppermute x53, waiting for transfers between devices, send(): return lax.ppermute(value, ('sp', 'tp'), pairs)  119 us
    ppermute x53, starting transfers between devices, send(): return lax.ppermute(value, ('sp', 'tp'), pairs)  57.9 us
    unnamed x58, local copies, waits for them, and re-layouts  10.2 us
    pallas_call x2, Pallas kernels, project(): pl.pallas_call(functools.partial(project_kernel, (nz, ny, nx, nc, rows, d...  6.23 us
  transfers between devices with their start and end apart: 53, of which 19 were waited for; matrix products, arithmetic and copies ran while one was open for 2% of the time, Pallas kernels for 5%

profile of v1, /device:TPU:0, one launch (start us, length us, event | category | flops | bytes accessed | tf_op | source)
XLA Modules:
  0.0 209.2 jit_solution(14656155771830341887)
XLA Ops:
  0.7 2.8 %pack.1 = (bf16[2,512,256]{2,1,0:T(8,128)(2,1)}, bf16[2,512,256]{2,1,0:T(8,128)(2,1)}, bf16[2,512,128]{2,1,0:T(8,128)(2,1)}, bf16[2,512,128]{2,1,0:T(8,128)(2,1)}) custom-call(s32[4]{0:T(128)} %pad_add_fusion.place, bf16[512,256]{1,0:T(8,128)(2,1)} %q1.1, bf16[512,256]{1,0:T(8,128)(2,1)} %q2.1, bf16[512,256]{1,0:T(8,128)(2,1)} %k1.1, bf16[512,256]{1,0:T(8,128)(2,1)} %k2.1, ...), custom_call_target="tpu_custom_call" | custom-call | flops 2097152 | bytes 2097152 | tf_op jit(solution)/shard_map/pack/pallas_call | solution.py:281
  4.0 3.1 %collective-permute-start.1 = (bf16[64,4096]{1,0:T(8,128)(2,1)S(1)}, bf16[64,4096]{1,0:T(8,128)(2,1)S(1)}, u32[]{:S(2)}, u32[]{:S(2)}) collective-permute-start(bf16[64,4096]{1,0:T(8,128)(2,1)S(1)} %copy-done), channel_id=1, source_target_pairs={{0,8},{1,9},{2,10},{3,11},{4,12},{5,13},{6,14},{7,15},{8,0},{9,1},... | collective-permute-start | bytes 1572872 | tf_op jit(solution)/shard_map/ppermute | solution.py:247
  10.4 2.5 %collective-permute-start.12 = (bf16[512,128]{1,0:T(8,128)(2,1)S(1)}, bf16[512,128]{1,0:T(8,128)(2,1)S(1)}, u32[]{:S(2)}, u32[]{:S(2)}) collective-permute-start(bf16[512,128]{1,0:T(8,128)(2,1)S(1)} %get-tuple-element.23), channel_id=1, source_target_pairs={{0,24},{1,25},{2,26},{3,27},{4,28},{5,29},{6,30},{7,31},{8,16},{9,... | collective-permute-start | bytes 393224 | tf_op jit(solution)/shard_map/ppermute | solution.py:247
  12.9 3.4 %collective-permute-start.11 = (bf16[512,128]{1,0:T(8,128)(2,1)S(1)}, bf16[512,128]{1,0:T(8,128)(2,1)S(1)}, u32[]{:S(2)}, u32[]{:S(2)}) collective-permute-start(bf16[512,128]{1,0:T(8,128)(2,1)S(1)} %get-tuple-element.22), channel_id=1, source_target_pairs={{0,16},{1,17},{2,18},{3,19},{4,20},{5,21},{6,22},{7,23},{8,24},{9,... | collective-permute-start | bytes 393224 | tf_op jit(solution)/shard_map/ppermute | solution.py:247
  17.2 8.1 %collective-permute-done.12 = bf16[512,128]{1,0:T(8,128)(2,1)S(1)} collective-permute-done((bf16[512,128]{1,0:T(8,128)(2,1)S(1)}, bf16[512,128]{1,0:T(8,128)(2,1)S(1)}, u32[]{:S(2)}, u32[]{:S(2)}) %collective-permute-start.12) | collective-permute-done | bytes 131104 | tf_op jit(solution)/shard_map/ppermute | solution.py:247
  28.0 6.6 %collective-permute-done.11 = bf16[512,128]{1,0:T(8,128)(2,1)S(1)} collective-permute-done((bf16[512,128]{1,0:T(8,128)(2,1)S(1)}, bf16[512,128]{1,0:T(8,128)(2,1)S(1)}, u32[]{:S(2)}, u32[]{:S(2)}) %collective-permute-start.11) | collective-permute-done | bytes 131104 | tf_op jit(solution)/shard_map/ppermute | solution.py:247
  34.6 4.8 %collective-permute-start.10 = (bf16[512,128]{1,0:T(8,128)(2,1)S(1)}, bf16[512,128]{1,0:T(8,128)(2,1)}, u32[]{:S(2)}, u32[]{:S(2)}) collective-permute-start(bf16[512,128]{1,0:T(8,128)(2,1)S(1)} %get-tuple-element.24), channel_id=1, source_target_pairs={{0,8},{1,9},{2,10},{3,11},{4,12},{5,13},{6,14},{7,15},{8,0},{9,1},... | collective-permute-start | bytes 393224 | tf_op jit(solution)/shard_map/ppermute | solution.py:247
  39.4 14.4 %collective-permute-done.10 = bf16[512,128]{1,0:T(8,128)(2,1)} collective-permute-done((bf16[512,128]{1,0:T(8,128)(2,1)S(1)}, bf16[512,128]{1,0:T(8,128)(2,1)}, u32[]{:S(2)}, u32[]{:S(2)}) %collective-permute-start.10) | collective-permute-done | bytes 131104 | tf_op jit(solution)/shard_map/ppermute | solution.py:247
  56.0 1.7 collective-permute-start.25
  57.8 3.8 %collective-permute-done.19.refs_10_ = bf16[512,256]{1,0:T(8,128)(2,1)S(1)} collective-permute-done((bf16[512,256]{1,0:T(8,128)(2,1)S(1)}, bf16[512,256]{1,0:T(8,128)(2,1)S(1)}, u32[]{:S(2)}, u32[]{:S(2)}) %collective-permute-start.19) | collective-permute-done | bytes 262176 | tf_op jit(solution)/shard_map/ppermute | solution.py:247
  63.1 3.7 %collective-permute-done.21.refs_12_ = bf16[512,256]{1,0:T(8,128)(2,1)S(1)} collective-permute-done((bf16[512,256]{1,0:T(8,128)(2,1)}, bf16[512,256]{1,0:T(8,128)(2,1)S(1)}, u32[]{:S(2)}, u32[]{:S(2)}) %collective-permute-start.21) | collective-permute-done | bytes 262176 | tf_op jit(solution)/shard_map/ppermute | solution.py:247
  68.3 9.2 %collective-permute-done.25.refs_16_ = bf16[512,256]{1,0:T(8,128)(2,1)S(1)} collective-permute-done((bf16[512,256]{1,0:T(8,128)(2,1)}, bf16[512,256]{1,0:T(8,128)(2,1)S(1)}, u32[]{:S(2)}, u32[]{:S(2)}) %collective-permute-start.25) | collective-permute-done | bytes 262176 | tf_op jit(solution)/shard_map/ppermute | solution.py:247
  81.3 1.6 collective-permute-start.27
  83.0 11.0 %collective-permute-done.7 = bf16[64,4096]{1,0:T(8,128)(2,1)S(1)} collective-permute-done((bf16[64,4096]{1,0:T(8,128)(2,1)}, bf16[64,4096]{1,0:T(8,128)(2,1)S(1)}, u32[]{:S(2)}, u32[]{:S(2)}) %collective-permute-start.7) | collective-permute-done | bytes 524320 | tf_op jit(solution)/shard_map/ppermute | solution.py:247
  97.3 4.1 %collective-permute-done.31.refs_22_ = bf16[512,256]{1,0:T(8,128)(2,1)S(1)} collective-permute-done((bf16[512,256]{1,0:T(8,128)(2,1)S(1)}, bf16[512,256]{1,0:T(8,128)(2,1)S(1)}, u32[]{:S(2)}, u32[]{:S(2)}) %collective-permute-start.31) | collective-permute-done | bytes 262176 | tf_op jit(solution)/shard_map/ppermute | solution.py:247
  107.2 2.3 %collective-permute-done.6.refs_5_ = bf16[64,4096]{1,0:T(8,128)(2,1)S(1)} collective-permute-done((bf16[64,4096]{1,0:T(8,128)(2,1)S(1)}, bf16[64,4096]{1,0:T(8,128)(2,1)S(1)}, u32[]{:S(2)}, u32[]{:S(2)}) %collective-permute-start.6) | collective-permute-done | bytes 524320 | tf_op jit(solution)/shard_map/ppermute | solution.py:247
  109.5 11.2 %collective-permute-done.8.refs_7_ = bf16[64,4096]{1,0:T(8,128)(2,1)S(1)} collective-permute-done((bf16[64,4096]{1,0:T(8,128)(2,1)S(1)}, bf16[64,4096]{1,0:T(8,128)(2,1)S(1)}, u32[]{:S(2)}, u32[]{:S(2)}) %collective-permute-start.8) | collective-permute-done | bytes 524320 | tf_op jit(solution)/shard_map/ppermute | solution.py:247
  121.4 3.1 %shard_map.92.refs_0_ = bf16[512,512]{1,0:T(8,128)(2,1)S(1)} custom-call(s32[4]{0:T(128)S(1)} %copy-done.20, f32[512,64]{1,0:T(8,128)S(1)} %get-tuple-element.28.cos_ref, f32[512,64]{1,0:T(8,128)S(1)} %get-tuple-element.27.sin_ref, bf16[64,4096]{1,0:T(8,128)(2,1)S(1)} %copy-done, bf16[64,4096]{1,0:T(8,128)(2,1)S(1)} %collective-permute-done.refs_1_, ...), custom_call_target="tpu_custom_call" | custom-call | flops 2147483648 | bytes 8388608 | tf_op jit(solution)/shard_map/pallas_call | solution.py:324
  127.5 2.5 %collective-permute-done.46.refs_12_ = bf16[512,512]{1,0:T(8,128)(2,1)S(1)} collective-permute-done((bf16[512,512]{1,0:T(8,128)(2,1)S(1)}, bf16[512,512]{1,0:T(8,128)(2,1)S(1)}, u32[]{:S(2)}, u32[]{:S(2)}) %collective-permute-start.46) | collective-permute-done | bytes 524320 | tf_op jit(solution)/shard_map/ppermute | solution.py:247
  132.0 8.9 %collective-permute-done.34.refs_2_ = bf16[512,512]{1,0:T(8,128)(2,1)S(1)} collective-permute-done((bf16[512,512]{1,0:T(8,128)(2,1)S(1)}, bf16[512,512]{1,0:T(8,128)(2,1)S(1)}, u32[]{:S(2)}, u32[]{:S(2)}) %collective-permute-start.34) | collective-permute-done | bytes 524320 | tf_op jit(solution)/shard_map/ppermute | solution.py:247
  141.4 10.3 %collective-permute-done.48.refs_14_ = bf16[512,512]{1,0:T(8,128)(2,1)S(1)} collective-permute-done((bf16[512,512]{1,0:T(8,128)(2,1)S(1)}, bf16[512,512]{1,0:T(8,128)(2,1)S(1)}, u32[]{:S(2)}, u32[]{:S(2)}) %collective-permute-start.48) | collective-permute-done | bytes 524320 | tf_op jit(solution)/shard_map/ppermute | solution.py:247
  152.3 3.1 %shard_map.91.q_ref = bf16[512,256]{1,0:T(8,128)(2,1)S(1)} custom-call(s32[4]{0:T(128)S(1)} %copy-done.20, f32[512,64]{1,0:T(8,128)S(1)} %get-tuple-element.28.cos_ref, f32[512,64]{1,0:T(8,128)S(1)} %get-tuple-element.27.sin_ref, bf16[64,4096]{1,0:T(8,128)(2,1)S(1)} %copy-done, bf16[64,4096]{1,0:T(8,128)(2,1)S(1)} %collective-permute-done.refs_1_, ...), custom_call_target="tpu_custom_call" | custom-call | flops 1073741824 | bytes 6291456 | tf_op jit(solution)/shard_map/pallas_call | solution.py:324
  156.1 3.8 %attend.1 = bf16[512,256]{1,0:T(8,128)(2,1)S(1)} custom-call(s32[4]{0:T(128)S(1)} %copy-done.20, bf16[512,256]{1,0:T(8,128)(2,1)S(1)} %shard_map.91.q_ref, f32[2]{0:T(128)S(1)} %copy-done.22, f32[2]{0:T(128)S(1)} %collective-permute-done.16.lam_other, f32[1,256]{1,0:T(1,128)S(1)} %bitcast.33, bf16[512,512]{1,0:T(8,128)(2,1)S(1)} %shard_map.92.refs_0_, ...), custom_call_target="tpu_custom_call" | custom-call | flops 1610612736 | bytes 2097152 | tf_op jit(solution)/shard_map/attend/pallas_call | solution.py:360
  163.6 2.4 %collective-permute-start.38 = (bf16[256,256]{1,0:T(8,128)(2,1)S(1)}, bf16[256,256]{1,0:T(8,128)(2,1)S(1)}, u32[]{:S(2)}, u32[]{:S(2)}) collective-permute-start(bf16[256,256]{1,0:T(8,128)(2,1)S(1)} %bitcast.30), channel_id=1, source_target_pairs={{0,24},{1,25},{2,26},{3,27},{4,28},{5,29},{6,30},{7,31},{8,16},{9,... | collective-permute-start | bytes 393224 | tf_op jit(solution)/shard_map/ppermute | solution.py:247
  169.3 2.7 %collective-permute-start.41 = (bf16[256,256]{1,0:T(8,128)(2,1)S(1)}, bf16[256,256]{1,0:T(8,128)(2,1)S(1)}, u32[]{:S(2)}, u32[]{:S(2)}) collective-permute-start(bf16[256,256]{1,0:T(8,128)(2,1)S(1)} %bitcast.36), channel_id=1, source_target_pairs={{0,18},{1,19},{2,16},{3,17},{4,22},{5,23},{6,20},{7,21},{8,26},{9,... | collective-permute-start | bytes 393224 | tf_op jit(solution)/shard_map/ppermute | solution.py:247
  172.0 2.9 %collective-permute-done.37.refs_2_ = bf16[256,256]{1,0:T(8,128)(2,1)S(1)} collective-permute-done((bf16[256,256]{1,0:T(8,128)(2,1)S(1)}, bf16[256,256]{1,0:T(8,128)(2,1)S(1)}, u32[]{:S(2)}, u32[]{:S(2)}) %collective-permute-start.37) | collective-permute-done | bytes 131104 | tf_op jit(solution)/shard_map/ppermute | solution.py:247
  174.9 2.4 %collective-permute-start.42 = (bf16[256,256]{1,0:T(8,128)(2,1)S(1)}, bf16[256,256]{1,0:T(8,128)(2,1)S(1)}, u32[]{:S(2)}, u32[]{:S(2)}) collective-permute-start(bf16[256,256]{1,0:T(8,128)(2,1)S(1)} %bitcast.37), channel_id=1, source_target_pairs={{0,26},{1,27},{2,24},{3,25},{4,30},{5,31},{6,28},{7,29},{8,18},{9,... | collective-permute-start | bytes 393224 | tf_op jit(solution)/shard_map/ppermute | solution.py:247
  177.8 9.0 %collective-permute-done.41.refs_6_ = bf16[256,256]{1,0:T(8,128)(2,1)S(1)} collective-permute-done((bf16[256,256]{1,0:T(8,128)(2,1)S(1)}, bf16[256,256]{1,0:T(8,128)(2,1)S(1)}, u32[]{:S(2)}, u32[]{:S(2)}) %collective-permute-start.41) | collective-permute-done | bytes 131104 | tf_op jit(solution)/shard_map/ppermute | solution.py:247
  191.0 1.8 out_project.1
  192.9 2.9 %collective-permute-start.50 = (bf16[64,1024]{1,0:T(8,128)(2,1)S(1)}, bf16[64,1024]{1,0:T(8,128)(2,1)S(1)}, u32[]{:S(2)}, u32[]{:S(2)}) collective-permute-start(bf16[64,1024]{1,0:T(8,128)(2,1)S(1)} %get-tuple-element.19), channel_id=1, source_target_pairs={{0,8},{1,9},{2,10},{3,11},{4,12},{5,13},{6,14},{7,15},{8,0},{9,1},... | collective-permute-start | bytes 393224 | tf_op jit(solution)/shard_map/ppermute | solution.py:247
  195.9 2.3 %collective-permute-start.52 = (bf16[64,1024]{1,0:T(8,128)(2,1)S(1)}, bf16[64,1024]{1,0:T(8,128)(2,1)S(1)}, u32[]{:S(2)}, u32[]{:S(2)}) collective-permute-start(bf16[64,1024]{1,0:T(8,128)(2,1)S(1)} %get-tuple-element.17), channel_id=1, source_target_pairs={{0,24},{1,25},{2,26},{3,27},{4,28},{5,29},{6,30},{7,31},{8,16},{9,... | collective-permute-start | bytes 393224 | tf_op jit(solution)/shard_map/ppermute | solution.py:247
  199.7 8.0 %collective-permute-done.51 = bf16[64,1024]{1,0:T(8,128)(2,1)S(1)} collective-permute-done((bf16[64,1024]{1,0:T(8,128)(2,1)S(1)}, bf16[64,1024]{1,0:T(8,128)(2,1)S(1)}, u32[]{:S(2)}, u32[]{:S(2)}) %collective-permute-start.51) | collective-permute-done | bytes 131104 | tf_op jit(solution)/shard_map/ppermute | solution.py:247
  (152 shorter events, 48.2 us)
Async XLA Ops:
  4.0 21.2 %collective-permute-start.1 = (bf16[64,4096]{1,0:T(8,128)(2,1)S(1)}, bf16[64,4096]{1,0:T(8,128)(2,1)S(1)}, u32[]{:S(2)}, u32[]{:S(2)}) collective-permute-start(bf16[64,4096]{1,0:T(8,128)(2,1)S(1)} %copy-done), channel_id=1, source_target_pairs={{0,8},{1,9},{2,10},{3,11},{4,12},{5,13},{6,14},{7,15},{8,0},{9,1},... | collective-permute-start | bytes 1572872 | tf_op jit(solution)/shard_map/ppermute | solution.py:247
  7.1 19.6 %collective-permute-start.4 = (bf16[64,4096]{1,0:T(8,128)(2,1)S(1)}, bf16[64,4096]{1,0:T(8,128)(2,1)S(1)}, u32[]{:S(2)}, u32[]{:S(2)}) collective-permute-start(bf16[64,4096]{1,0:T(8,128)(2,1)S(1)} %copy-done), channel_id=1, source_target_pairs={{8,16},{9,17},{10,18},{11,19},{12,20},{13,21},{14,22},{15,23},{16,... | collective-permute-start | bytes 1572872 | tf_op jit(solution)/shard_map/ppermute | solution.py:247
  7.8 47.5 %collective-permute-start = (bf16[64,4096]{1,0:T(8,128)(2,1)S(1)}, bf16[64,4096]{1,0:T(8,128)(2,1)S(1)}, u32[]{:S(2)}, u32[]{:S(2)}) collective-permute-start(bf16[64,4096]{1,0:T(8,128)(2,1)S(1)} %copy-done), channel_id=1, source_target_pairs={{0,2},{1,3},{2,0},{3,1},{4,6},{5,7},{6,4},{7,5},{8,10},{9,11},{10,... | collective-permute-start | bytes 1572872 | tf_op jit(solution)/shard_map/ppermute | solution.py:247
  10.4 14.8 %collective-permute-start.12 = (bf16[512,128]{1,0:T(8,128)(2,1)S(1)}, bf16[512,128]{1,0:T(8,128)(2,1)S(1)}, u32[]{:S(2)}, u32[]{:S(2)}) collective-permute-start(bf16[512,128]{1,0:T(8,128)(2,1)S(1)} %get-tuple-element.23), channel_id=1, source_target_pairs={{0,24},{1,25},{2,26},{3,27},{4,28},{5,29},{6,30},{7,31},{8,16},{9,... | collective-permute-start | bytes 393224 | tf_op jit(solution)/shard_map/ppermute | solution.py:247
  12.9 21.7 %collective-permute-start.11 = (bf16[512,128]{1,0:T(8,128)(2,1)S(1)}, bf16[512,128]{1,0:T(8,128)(2,1)S(1)}, u32[]{:S(2)}, u32[]{:S(2)}) collective-permute-start(bf16[512,128]{1,0:T(8,128)(2,1)S(1)} %get-tuple-element.22), channel_id=1, source_target_pairs={{0,16},{1,17},{2,18},{3,19},{4,20},{5,21},{6,22},{7,23},{8,24},{9,... | collective-permute-start | bytes 393224 | tf_op jit(solution)/shard_map/ppermute | solution.py:247
  25.2 30.1 %collective-permute-start.18 = (bf16[512,256]{1,0:T(8,128)(2,1)S(1)}, bf16[512,256]{1,0:T(8,128)(2,1)S(1)}, u32[]{:S(2)}, u32[]{:S(2)}) collective-permute-start(bf16[512,256]{1,0:T(8,128)(2,1)S(1)} %get-tuple-element.16.refs_8_), channel_id=1, source_target_pairs={{0,1},{1,0},{2,3},{3,2},{4,5},{5,4},{6,7},{7,6},{8,9},{9,8},{10,11... | collective-permute-start | bytes 786440 | tf_op jit(solution)/shard_map/ppermute | solution.py:247
  25.2 52.3 %collective-permute-start.3 = (bf16[64,4096]{1,0:T(8,128)(2,1)S(1)}, bf16[64,4096]{1,0:T(8,128)(2,1)}, u32[]{:S(2)}, u32[]{:S(2)}) collective-permute-start(bf16[64,4096]{1,0:T(8,128)(2,1)S(1)} %collective-permute-done.1.refs_2_), channel_id=1, source_target_pairs={{8,16},{9,17},{10,18},{11,19},{12,20},{13,21},{14,22},{15,23},{16,... | collective-permute-start | bytes 1572872 | tf_op jit(solution)/shard_map/ppermute | solution.py:247
  26.7 51.4 %collective-permute-start.5 = (bf16[64,4096]{1,0:T(8,128)(2,1)S(1)}, bf16[64,4096]{1,0:T(8,128)(2,1)}, u32[]{:S(2)}, u32[]{:S(2)}) collective-permute-start(bf16[64,4096]{1,0:T(8,128)(2,1)S(1)} %collective-permute-done.4), channel_id=1, source_target_pairs={{8,0},{9,1},{10,2},{11,3},{12,4},{13,5},{14,6},{15,7},{16,24},{17,... | collective-permute-start | bytes 1572872 | tf_op jit(solution)/shard_map/ppermute | solution.py:247
  34.6 19.2 %collective-permute-start.10 = (bf16[512,128]{1,0:T(8,128)(2,1)S(1)}, bf16[512,128]{1,0:T(8,128)(2,1)}, u32[]{:S(2)}, u32[]{:S(2)}) collective-permute-start(bf16[512,128]{1,0:T(8,128)(2,1)S(1)} %get-tuple-element.24), channel_id=1, source_target_pairs={{0,8},{1,9},{2,10},{3,11},{4,12},{5,13},{6,14},{7,15},{8,0},{9,1},... | collective-permute-start | bytes 393224 | tf_op jit(solution)/shard_map/ppermute | solution.py:247
  56.0 21.5 %collective-permute-start.25 = (bf16[512,256]{1,0:T(8,128)(2,1)}, bf16[512,256]{1,0:T(8,128)(2,1)S(1)}, u32[]{:S(2)}, u32[]{:S(2)}) collective-permute-start(bf16[512,256]{1,0:T(8,128)(2,1)} %get-tuple-element.14), channel_id=1, source_target_pairs={{0,16},{1,17},{2,18},{3,19},{4,20},{5,21},{6,22},{7,23},{8,24},{9,... | collective-permute-start | bytes 786440 | tf_op jit(solution)/shard_map/ppermute | solution.py:247
  61.6 19.1 %collective-permute-start.29 = (bf16[512,256]{1,0:T(8,128)(2,1)S(1)}, bf16[512,256]{1,0:T(8,128)(2,1)S(1)}, u32[]{:S(2)}, u32[]{:S(2)}) collective-permute-start(bf16[512,256]{1,0:T(8,128)(2,1)S(1)} %get-tuple-element.13), channel_id=1, source_target_pairs={{0,24},{1,25},{2,26},{3,27},{4,28},{5,29},{6,30},{7,31},{8,16},{9,... | collective-permute-start | bytes 786440 | tf_op jit(solution)/shard_map/ppermute | solution.py:247
  66.8 14.4 %collective-permute-start.2 = (bf16[64,4096]{1,0:T(8,128)(2,1)S(1)}, bf16[64,4096]{1,0:T(8,128)(2,1)S(1)}, u32[]{:S(2)}, u32[]{:S(2)}) collective-permute-start(bf16[64,4096]{1,0:T(8,128)(2,1)S(1)} %collective-permute-done.1.refs_2_), channel_id=1, source_target_pairs={{0,2},{1,3},{2,0},{3,1},{4,6},{5,7},{6,4},{7,5},{8,10},{9,11},{10,... | collective-permute-start | bytes 1572872 | tf_op jit(solution)/shard_map/ppermute | solution.py:247
  78.1 16.0 %collective-permute-start.7 = (bf16[64,4096]{1,0:T(8,128)(2,1)}, bf16[64,4096]{1,0:T(8,128)(2,1)S(1)}, u32[]{:S(2)}, u32[]{:S(2)}) collective-permute-start(bf16[64,4096]{1,0:T(8,128)(2,1)} %collective-permute-done.3), channel_id=1, source_target_pairs={{8,0},{9,1},{10,2},{11,3},{12,4},{13,5},{14,6},{15,7},{16,24},{17,... | collective-permute-start | bytes 1572872 | tf_op jit(solution)/shard_map/ppermute | solution.py:247
  80.7 14.0 %collective-permute-start.23 = (bf16[512,256]{1,0:T(8,128)(2,1)S(1)}, bf16[512,256]{1,0:T(8,128)(2,1)S(1)}, u32[]{:S(2)}, u32[]{:S(2)}) collective-permute-start(bf16[512,256]{1,0:T(8,128)(2,1)S(1)} %collective-permute-done.21.refs_12_), channel_id=1, source_target_pairs={{0,4},{1,5},{2,6},{3,7},{4,0},{5,1},{6,2},{7,3},{8,12},{9,13},{10,... | collective-permute-start | bytes 786440 | tf_op jit(solution)/shard_map/ppermute | solution.py:247
  81.3 15.0 %collective-permute-start.26 = (bf16[512,256]{1,0:T(8,128)(2,1)S(1)}, bf16[512,256]{1,0:T(8,128)(2,1)S(1)}, u32[]{:S(2)}, u32[]{:S(2)}) collective-permute-start(bf16[512,256]{1,0:T(8,128)(2,1)S(1)} %collective-permute-done.25.refs_16_), channel_id=1, source_target_pairs={{0,1},{1,0},{2,3},{3,2},{4,5},{5,4},{6,7},{7,6},{8,9},{9,8},{10,11... | collective-permute-start | bytes 786440 | tf_op jit(solution)/shard_map/ppermute | solution.py:247
  81.3 15.5 %collective-permute-start.27 = (bf16[512,256]{1,0:T(8,128)(2,1)S(1)}, bf16[512,256]{1,0:T(8,128)(2,1)S(1)}, u32[]{:S(2)}, u32[]{:S(2)}) collective-permute-start(bf16[512,256]{1,0:T(8,128)(2,1)S(1)} %collective-permute-done.25.refs_16_), channel_id=1, source_target_pairs={{0,4},{1,5},{2,6},{3,7},{4,0},{5,1},{6,2},{7,3},{8,12},{9,13},{10,... | collective-permute-start | bytes 786440 | tf_op jit(solution)/shard_map/ppermute | solution.py:247
  82.9 14.0 %collective-permute-start.30 = (bf16[512,256]{1,0:T(8,128)(2,1)S(1)}, bf16[512,256]{1,0:T(8,128)(2,1)S(1)}, u32[]{:S(2)}, u32[]{:S(2)}) collective-permute-start(bf16[512,256]{1,0:T(8,128)(2,1)S(1)} %collective-permute-done.29.refs_20_), channel_id=1, source_target_pairs={{0,1},{1,0},{2,3},{3,2},{4,5},{5,4},{6,7},{7,6},{8,9},{9,8},{10,11... | collective-permute-start | bytes 786440 | tf_op jit(solution)/shard_map/ppermute | solution.py:247
  94.7 14.9 %collective-permute-start.6 = (bf16[64,4096]{1,0:T(8,128)(2,1)S(1)}, bf16[64,4096]{1,0:T(8,128)(2,1)S(1)}, u32[]{:S(2)}, u32[]{:S(2)}) collective-permute-start(bf16[64,4096]{1,0:T(8,128)(2,1)S(1)} %broadcast_select_fusion.1.refs_4_), channel_id=1, source_target_pairs={{0,2},{1,3},{2,0},{3,1},{4,6},{5,7},{6,4},{7,5},{8,10},{9,11},{10,... | collective-permute-start | bytes 1572872 | tf_op jit(solution)/shard_map/ppermute | solution.py:247
  96.2 24.5 %collective-permute-start.8 = (bf16[64,4096]{1,0:T(8,128)(2,1)S(1)}, bf16[64,4096]{1,0:T(8,128)(2,1)S(1)}, u32[]{:S(2)}, u32[]{:S(2)}) collective-permute-start(bf16[64,4096]{1,0:T(8,128)(2,1)S(1)} %broadcast_select_fusion.refs_6_), channel_id=1, source_target_pairs={{0,2},{1,3},{2,0},{3,1},{4,6},{5,7},{6,4},{7,5},{8,10},{9,11},{10,... | collective-permute-start | bytes 1572872 | tf_op jit(solution)/shard_map/ppermute | solution.py:247
  103.6 27.9 %collective-permute-start.44 = (bf16[512,512]{1,0:T(8,128)(2,1)S(1)}, bf16[512,512]{1,0:T(8,128)(2,1)S(1)}, u32[]{:S(2)}, u32[]{:S(2)}) collective-permute-start(bf16[512,512]{1,0:T(8,128)(2,1)S(1)} %copy-done.1), channel_id=1, source_target_pairs={{0,4},{1,5},{2,6},{3,7},{4,0},{5,1},{6,2},{7,3},{8,12},{9,13},{10,... | collective-permute-start | bytes 1572872 | tf_op jit(solution)/shard_map/ppermute | solution.py:247
  104.1 25.8 %collective-permute-start.46 = (bf16[512,512]{1,0:T(8,128)(2,1)S(1)}, bf16[512,512]{1,0:T(8,128)(2,1)S(1)}, u32[]{:S(2)}, u32[]{:S(2)}) collective-permute-start(bf16[512,512]{1,0:T(8,128)(2,1)S(1)} %copy-done.1), channel_id=1, source_target_pairs={{0,2},{1,3},{2,0},{3,1},{4,6},{5,7},{6,4},{7,5},{8,10},{9,11},{10,... | collective-permute-start | bytes 1572872 | tf_op jit(solution)/shard_map/ppermute | solution.py:247
  105.6 25.8 %collective-permute-start.14 = (bf16[2048,128]{1,0:T(8,128)(2,1)S(1)}, bf16[2048,128]{1,0:T(8,128)(2,1)S(1)}, u32[]{:S(2)}, u32[]{:S(2)}) collective-permute-start(bf16[2048,128]{1,0:T(8,128)(2,1)S(1)} %pad_maximum_fusion.refs_8_), channel_id=1, source_target_pairs={{0,4},{1,5},{2,6},{3,7},{4,0},{5,1},{6,2},{7,3},{8,12},{9,13},{10,... | collective-permute-start | bytes 1572872 | tf_op jit(solution)/shard_map/ppermute | solution.py:247
  124.6 16.3 %collective-permute-start.34 = (bf16[512,512]{1,0:T(8,128)(2,1)S(1)}, bf16[512,512]{1,0:T(8,128)(2,1)S(1)}, u32[]{:S(2)}, u32[]{:S(2)}) collective-permute-start(bf16[512,512]{1,0:T(8,128)(2,1)S(1)} %shard_map.92.refs_0_), channel_id=1, source_target_pairs={{0,4},{1,5},{2,6},{3,7},{4,0},{5,1},{6,2},{7,3},{8,12},{9,13},{10,... | collective-permute-start | bytes 1572872 | tf_op jit(solution)/shard_map/ppermute | solution.py:247
  129.9 21.7 %collective-permute-start.48 = (bf16[512,512]{1,0:T(8,128)(2,1)S(1)}, bf16[512,512]{1,0:T(8,128)(2,1)S(1)}, u32[]{:S(2)}, u32[]{:S(2)}) collective-permute-start(bf16[512,512]{1,0:T(8,128)(2,1)S(1)} %collective-permute-done.46.refs_12_), channel_id=1, source_target_pairs={{0,4},{1,5},{2,6},{3,7},{4,0},{5,1},{6,2},{7,3},{8,12},{9,13},{10,... | collective-permute-start | bytes 1572872 | tf_op jit(solution)/shard_map/ppermute | solution.py:247
  131.5 20.2 %collective-permute-start.15 = (bf16[2048,128]{1,0:T(8,128)(2,1)S(1)}, bf16[2048,128]{1,0:T(8,128)(2,1)S(1)}, u32[]{:S(2)}, u32[]{:S(2)}) collective-permute-start(bf16[2048,128]{1,0:T(8,128)(2,1)S(1)} %collective-permute-done.14.refs_10_), channel_id=1, source_target_pairs={{0,1},{1,0},{2,3},{3,2},{4,5},{5,4},{6,7},{7,6},{8,9},{9,8},{10,11... | collective-permute-start | bytes 1572872 | tf_op jit(solution)/shard_map/ppermute | solution.py:247
  131.5 20.7 %collective-permute-start.33 = (bf16[512,512]{1,0:T(8,128)(2,1)S(1)}, bf16[512,512]{1,0:T(8,128)(2,1)S(1)}, u32[]{:S(2)}, u32[]{:S(2)}) collective-permute-start(bf16[512,512]{1,0:T(8,128)(2,1)S(1)} %shard_map.92.refs_0_), channel_id=1, source_target_pairs={{0,1},{1,0},{2,3},{3,2},{4,5},{5,4},{6,7},{7,6},{8,9},{9,8},{10,11... | collective-permute-start | bytes 1572872 | tf_op jit(solution)/shard_map/ppermute | solution.py:247
  140.9 14.5 %collective-permute-start.35 = (bf16[512,512]{1,0:T(8,128)(2,1)S(1)}, bf16[512,512]{1,0:T(8,128)(2,1)S(1)}, u32[]{:S(2)}, u32[]{:S(2)}) collective-permute-start(bf16[512,512]{1,0:T(8,128)(2,1)S(1)} %collective-permute-done.34.refs_2_), channel_id=1, source_target_pairs={{0,1},{1,0},{2,3},{3,2},{4,5},{5,4},{6,7},{7,6},{8,9},{9,8},{10,11... | collective-permute-start | bytes 1572872 | tf_op jit(solution)/shard_map/ppermute | solution.py:247
  140.9 20.3 %collective-permute-start.43 = (bf16[512,512]{1,0:T(8,128)(2,1)S(1)}, bf16[512,512]{1,0:T(8,128)(2,1)S(1)}, u32[]{:S(2)}, u32[]{:S(2)}) collective-permute-start(bf16[512,512]{1,0:T(8,128)(2,1)S(1)} %copy-done.1), channel_id=1, source_target_pairs={{0,1},{1,0},{2,3},{3,2},{4,5},{5,4},{6,7},{7,6},{8,9},{9,8},{10,11... | collective-permute-start | bytes 1572872 | tf_op jit(solution)/shard_map/ppermute | solution.py:247
  151.7 14.3 %collective-permute-start.47 = (bf16[512,512]{1,0:T(8,128)(2,1)S(1)}, bf16[512,512]{1,0:T(8,128)(2,1)S(1)}, u32[]{:S(2)}, u32[]{:S(2)}) collective-permute-start(bf16[512,512]{1,0:T(8,128)(2,1)S(1)} %collective-permute-done.46.refs_12_), channel_id=1, source_target_pairs={{0,1},{1,0},{2,3},{3,2},{4,5},{5,4},{6,7},{7,6},{8,9},{9,8},{10,11... | collective-permute-start | bytes 1572872 | tf_op jit(solution)/shard_map/ppermute | solution.py:247
  152.2 16.1 %collective-permute-start.49 = (bf16[512,512]{1,0:T(8,128)(2,1)S(1)}, bf16[512,512]{1,0:T(8,128)(2,1)S(1)}, u32[]{:S(2)}, u32[]{:S(2)}) collective-permute-start(bf16[512,512]{1,0:T(8,128)(2,1)S(1)} %collective-permute-done.48.refs_14_), channel_id=1, source_target_pairs={{0,1},{1,0},{2,3},{3,2},{4,5},{5,4},{6,7},{7,6},{8,9},{9,8},{10,11... | collective-permute-start | bytes 1572872 | tf_op jit(solution)/shard_map/ppermute | solution.py:247
  163.6 13.7 %collective-permute-start.38 = (bf16[256,256]{1,0:T(8,128)(2,1)S(1)}, bf16[256,256]{1,0:T(8,128)(2,1)S(1)}, u32[]{:S(2)}, u32[]{:S(2)}) collective-permute-start(bf16[256,256]{1,0:T(8,128)(2,1)S(1)} %bitcast.30), channel_id=1, source_target_pairs={{0,24},{1,25},{2,26},{3,27},{4,28},{5,29},{6,30},{7,31},{8,16},{9,... | collective-permute-start | bytes 393224 | tf_op jit(solution)/shard_map/ppermute | solution.py:247
  169.3 17.5 %collective-permute-start.41 = (bf16[256,256]{1,0:T(8,128)(2,1)S(1)}, bf16[256,256]{1,0:T(8,128)(2,1)S(1)}, u32[]{:S(2)}, u32[]{:S(2)}) collective-permute-start(bf16[256,256]{1,0:T(8,128)(2,1)S(1)} %bitcast.36), channel_id=1, source_target_pairs={{0,18},{1,19},{2,16},{3,17},{4,22},{5,23},{6,20},{7,21},{8,26},{9,... | collective-permute-start | bytes 393224 | tf_op jit(solution)/shard_map/ppermute | solution.py:247
  (50 other events, 413.9 us)

commit v2 on v1

--- a/solution.py
+++ b/solution.py
@@ -51,9 +51,10 @@
 
 
 def project_kernel(dims, place, cos_ref, sin_ref, *refs):
-    nz, ny, nx, nc, _, depth, qk, windows, stacked = dims
+    nz, ny, nx, nc, _, depth, qk, windows = dims
     tokens = refs[: nz * nx]
     weights = refs[nz * nx : -2]
+    per = nz * ny * nc // len(weights)
     out_ref, acc = refs[-2:]
     z, y = place[0], place[1]
     low, high = windows[0][0], windows[-1][1]
@@ -63,10 +64,8 @@
             cols = pl.ds(pl.multiple_of(start, depth), depth)
             left = jnp.concatenate([t[:, cols] for t in tokens], axis=0)
             for kc in range(nc):
-                if stacked:
-                    right = weights[ky * nc + kc][r * depth : (r + 1) * depth, low:high]
-                else:
-                    right = weights[(r * ny + ky) * nc + kc][:, low:high]
+                first = r % per * depth
+                right = weights[(r // per * ny + ky) * nc + kc][first : first + depth, low:high]
                 part = jnp.dot(left, right, preferred_element_type=jnp.float32)
                 if r or ky:
                     part = part + acc[kc]
@@ -87,7 +86,7 @@
 def attend_kernel(dims, place, q_ref, lam_own, lam_other, gain_ref, *refs):
     nz, ny, nx, nc, rows, qk, v = dims
     pieces = refs[: ny * nc]
-    out_ref, kv_all, s_all = refs[ny * nc :]
+    out_refs, (kv_all, s_all) = refs[ny * nc : -2], refs[-2:]
     z, y, x, c = (place[i] for i in range(4))
     tile = nx * rows
     block = ny * nc * tile
@@ -171,7 +170,9 @@
         )
         mean = jnp.mean(mixed * mixed, axis=-1, keepdims=True)
         scaled = mixed * lax.rsqrt(mean + EPS_NORM) * gain_ref[...]
-        out_ref[t * tile : (t + 1) * tile, :] = scaled.astype(jnp.bfloat16)
+        done = scaled.astype(jnp.bfloat16)
+        for k in range(nx):
+            out_refs[k][t * rows : (t + 1) * rows, :] = done[k * rows : (k + 1) * rows, :]
 
 
 def out_kernel(dims, place, *refs):
@@ -300,12 +301,13 @@
     for r in range(nz):
         own_core = (z ^ r) // hp == c
         q_rows.append(from_z(jnp.where(own_core, keep_q[r % hp], taken_q[r % hp]), r))
-    q_rows = jnp.concatenate(q_rows, axis=0)
     q_pieces = []
-    for ky in range(ny):
-        beside = from_y(q_rows, ky)
-        for kc in range(nc):
-            q_pieces.append(from_c(beside, kc))
+    for g in range(2):
+        group = jnp.concatenate(q_rows[g * nz // 2 : (g + 1) * nz // 2], axis=0)
+        for ky in range(ny):
+            beside = from_y(group, ky)
+            for kc in range(nc):
+                q_pieces.append(from_c(beside, kc))
 
     index = jnp.arange(nz * nx * rows, dtype=jnp.int32)
     at_z = z ^ (index // (nx * rows))
@@ -320,9 +322,8 @@
 
     def project(windows, weights):
         wide = sum(last - first for first, last, _ in windows)
-        stacked = len(weights) < nz * ny * nc
         return pl.pallas_call(
-            functools.partial(project_kernel, (nz, ny, nx, nc, rows, depth, qk, windows, stacked)),
+            functools.partial(project_kernel, (nz, ny, nx, nc, rows, depth, qk, windows)),
             out_shape=jax.ShapeDtypeStruct((total_rows, nc * wide), jnp.bfloat16),
             in_specs=[SMEM] + [VMEM] * (2 + nz * nx + len(weights)),
             out_specs=VMEM,
@@ -359,9 +360,9 @@
     pairs = total_rows * total_rows * ny * nc
     attended = pl.pallas_call(
         functools.partial(attend_kernel, (nz, ny, nx, nc, rows, qk, v)),
-        out_shape=jax.ShapeDtypeStruct((total_rows, v), jnp.bfloat16),
+        out_shape=(jax.ShapeDtypeStruct((nz * rows, v), jnp.bfloat16),) * nx,
         in_specs=[SMEM, VMEM, SMEM, SMEM, VMEM] + [VMEM] * (ny * nc),
-        out_specs=VMEM,
+        out_specs=(VMEM,) * nx,
         scratch_shapes=[
             pltpu.VMEM((ny * nc * total_rows, 2 * qk + v), jnp.bfloat16),
             pltpu.VMEM((nx * rows, ny * nc * total_rows), jnp.float32),
@@ -379,10 +380,9 @@
         name="attend",
     )(place, q, lambdas, lam_other, head_gain.reshape(1, v), *kv_pieces)
 
-    attended = attended.reshape(nz, nx, rows, v)
     chunks = []
     for k in range(nx):
-        mine = attended[:, k].reshape(nz * rows, v)
+        mine = attended[k]
         for r in range(nz):
             chunks.append(
                 send(mine, lambda a, b, d, e, k=k, r=r: (a ^ r, b, (d + k) % nx, e))

time: 210 us -> 206 us (0.981)
  waiting for transfers between devices: 119 us -> 116 us
    ppermute x53 -> x56, waiting for transfers between devices: 119 us -> 116 us  [send(): return lax.ppermute(value, ('sp', 'tp'), pairs)]
    ppermute x53 -> x56, starting transfers between devices: 57.9 us -> 57.7 us  [send(): return lax.ppermute(value, ('sp', 'tp'), pairs)]
    unnamed x58 -> x57, local copies, waits for them, and re-layouts: 10.2 us -> 10.2 us
  transfers between devices with their start and end apart: 53 -> 56, of which waited for: 19 -> 19; matrix products, arithmetic and copies ran while one was open for 2% -> 3% of each run, Pallas kernels for 5% -> 5%
where the time goes in v2:
time: 206 us
  waiting for transfers between devices  116 us (56%)
  starting transfers between devices  57.7 us (28%)
  Pallas kernels  14.7 us (7%)
  local copies, waits for them, and re-layouts  11 us (5%)
  other arithmetic  6.54 us (3%)
    ppermute x56, waiting for transfers between devices, send(): return lax.ppermute(value, ('sp', 'tp'), pairs)  116 us
    ppermute x56, starting transfers between devices, send(): return lax.ppermute(value, ('sp', 'tp'), pairs)  57.7 us
    unnamed x57, local copies, waits for them, and re-layouts  10.2 us
    pallas_call x2, Pallas kernels, project(): pl.pallas_call(functools.partial(project_kernel, (nz, ny, nx, nc, rows, d...  6.23 us
  transfers between devices with their start and end apart: 56, of which 19 were waited for; matrix products, arithmetic and copies ran while one was open for 3% of the time, Pallas kernels for 5%

profile of v2, /device:TPU:0, one launch (start us, length us, event | category | flops | bytes accessed | tf_op | source)
XLA Modules:
  0.0 205.9 jit_solution(14555864491225904106)
XLA Ops:
  0.6 2.8 %pack.1 = (bf16[2,512,256]{2,1,0:T(8,128)(2,1)}, bf16[2,512,256]{2,1,0:T(8,128)(2,1)}, bf16[2,512,128]{2,1,0:T(8,128)(2,1)}, bf16[2,512,128]{2,1,0:T(8,128)(2,1)}) custom-call(s32[4]{0:T(128)} %pad_add_fusion.place, bf16[512,256]{1,0:T(8,128)(2,1)} %q1.1, bf16[512,256]{1,0:T(8,128)(2,1)} %q2.1, bf16[512,256]{1,0:T(8,128)(2,1)} %k1.1, bf16[512,256]{1,0:T(8,128)(2,1)} %k2.1, ...), custom_call_target="tpu_custom_call" | custom-call | flops 2097152 | bytes 2097152 | tf_op jit(solution)/shard_map/pack/pallas_call | solution.py:282
  3.9 2.6 %collective-permute-start.1 = (bf16[64,4096]{1,0:T(8,128)(2,1)S(1)}, bf16[64,4096]{1,0:T(8,128)(2,1)S(1)}, u32[]{:S(2)}, u32[]{:S(2)}) collective-permute-start(bf16[64,4096]{1,0:T(8,128)(2,1)S(1)} %copy-done), channel_id=1, source_target_pairs={{0,8},{1,9},{2,10},{3,11},{4,12},{5,13},{6,14},{7,15},{8,0},{9,1},... | collective-permute-start | bytes 1572872 | tf_op jit(solution)/shard_map/ppermute | solution.py:248
  8.8 2.0 select_bitcast_fusion
  11.3 7.8 %collective-permute-done.1.refs_2_ = bf16[64,4096]{1,0:T(8,128)(2,1)S(1)} collective-permute-done((bf16[64,4096]{1,0:T(8,128)(2,1)S(1)}, bf16[64,4096]{1,0:T(8,128)(2,1)S(1)}, u32[]{:S(2)}, u32[]{:S(2)}) %collective-permute-start.1) | collective-permute-done | bytes 524320 | tf_op jit(solution)/shard_map/ppermute | solution.py:248
  22.6 4.6 %collective-permute-start.10 = (bf16[512,128]{1,0:T(8,128)(2,1)S(1)}, bf16[512,128]{1,0:T(8,128)(2,1)}, u32[]{:S(2)}, u32[]{:S(2)}) collective-permute-start(bf16[512,128]{1,0:T(8,128)(2,1)S(1)} %get-tuple-element.27), channel_id=1, source_target_pairs={{0,8},{1,9},{2,10},{3,11},{4,12},{5,13},{6,14},{7,15},{8,0},{9,1},... | collective-permute-start | bytes 393224 | tf_op jit(solution)/shard_map/ppermute | solution.py:248
  27.2 12.7 %collective-permute-done.10 = bf16[512,128]{1,0:T(8,128)(2,1)} collective-permute-done((bf16[512,128]{1,0:T(8,128)(2,1)S(1)}, bf16[512,128]{1,0:T(8,128)(2,1)}, u32[]{:S(2)}, u32[]{:S(2)}) %collective-permute-start.10) | collective-permute-done | bytes 131104 | tf_op jit(solution)/shard_map/ppermute | solution.py:248
  42.2 3.2 %collective-permute-start.28 = (bf16[512,256]{1,0:T(8,128)(2,1)}, bf16[512,256]{1,0:T(8,128)(2,1)S(1)}, u32[]{:S(2)}, u32[]{:S(2)}) collective-permute-start(bf16[512,256]{1,0:T(8,128)(2,1)} %get-tuple-element.18), channel_id=1, source_target_pairs={{0,16},{1,17},{2,18},{3,19},{4,20},{5,21},{6,22},{7,23},{8,24},{9,... | collective-permute-start | bytes 786440 | tf_op jit(solution)/shard_map/ppermute | solution.py:248
  46.9 2.6 %collective-permute-start.32 = (bf16[512,256]{1,0:T(8,128)(2,1)S(1)}, bf16[512,256]{1,0:T(8,128)(2,1)S(1)}, u32[]{:S(2)}, u32[]{:S(2)}) collective-permute-start(bf16[512,256]{1,0:T(8,128)(2,1)S(1)} %copy-done.24), channel_id=1, source_target_pairs={{0,24},{1,25},{2,26},{3,27},{4,28},{5,29},{6,30},{7,31},{8,16},{9,... | collective-permute-start | bytes 786440 | tf_op jit(solution)/shard_map/ppermute | solution.py:248
  49.5 2.8 %collective-permute-done.24.refs_12_ = bf16[512,256]{1,0:T(8,128)(2,1)S(1)} collective-permute-done((bf16[512,256]{1,0:T(8,128)(2,1)}, bf16[512,256]{1,0:T(8,128)(2,1)S(1)}, u32[]{:S(2)}, u32[]{:S(2)}) %collective-permute-start.24) | collective-permute-done | bytes 262176 | tf_op jit(solution)/shard_map/ppermute | solution.py:248
  53.8 10.1 %collective-permute-done.28.refs_16_ = bf16[512,256]{1,0:T(8,128)(2,1)S(1)} collective-permute-done((bf16[512,256]{1,0:T(8,128)(2,1)}, bf16[512,256]{1,0:T(8,128)(2,1)S(1)}, u32[]{:S(2)}, u32[]{:S(2)}) %collective-permute-start.28) | collective-permute-done | bytes 262176 | tf_op jit(solution)/shard_map/ppermute | solution.py:248
  67.6 1.6 collective-permute-start.30
  69.4 11.0 %collective-permute-done.7 = bf16[64,4096]{1,0:T(8,128)(2,1)S(1)} collective-permute-done((bf16[64,4096]{1,0:T(8,128)(2,1)}, bf16[64,4096]{1,0:T(8,128)(2,1)S(1)}, u32[]{:S(2)}, u32[]{:S(2)}) %collective-permute-start.7) | collective-permute-done | bytes 524320 | tf_op jit(solution)/shard_map/ppermute | solution.py:248
  83.8 4.0 %collective-permute-done.34.refs_22_ = bf16[512,256]{1,0:T(8,128)(2,1)S(1)} collective-permute-done((bf16[512,256]{1,0:T(8,128)(2,1)S(1)}, bf16[512,256]{1,0:T(8,128)(2,1)S(1)}, u32[]{:S(2)}, u32[]{:S(2)}) %collective-permute-start.34) | collective-permute-done | bytes 262176 | tf_op jit(solution)/shard_map/ppermute | solution.py:248
  92.0 3.9 %collective-permute-done.6.refs_5_ = bf16[64,4096]{1,0:T(8,128)(2,1)S(1)} collective-permute-done((bf16[64,4096]{1,0:T(8,128)(2,1)S(1)}, bf16[64,4096]{1,0:T(8,128)(2,1)S(1)}, u32[]{:S(2)}, u32[]{:S(2)}) %collective-permute-start.6) | collective-permute-done | bytes 524320 | tf_op jit(solution)/shard_map/ppermute | solution.py:248
  95.9 11.2 %collective-permute-done.8.refs_7_ = bf16[64,4096]{1,0:T(8,128)(2,1)S(1)} collective-permute-done((bf16[64,4096]{1,0:T(8,128)(2,1)S(1)}, bf16[64,4096]{1,0:T(8,128)(2,1)S(1)}, u32[]{:S(2)}, u32[]{:S(2)}) %collective-permute-start.8) | collective-permute-done | bytes 524320 | tf_op jit(solution)/shard_map/ppermute | solution.py:248
  107.1 1.8 collective-permute-start.15
  109.5 3.1 %shard_map.92.refs_0_ = bf16[512,512]{1,0:T(8,128)(2,1)S(1)} custom-call(s32[4]{0:T(128)S(1)} %copy-done.20, f32[512,64]{1,0:T(8,128)S(1)} %get-tuple-element.30.cos_ref, f32[512,64]{1,0:T(8,128)S(1)} %get-tuple-element.29.sin_ref, bf16[64,4096]{1,0:T(8,128)(2,1)S(1)} %copy-done, bf16[64,4096]{1,0:T(8,128)(2,1)S(1)} %collective-permute-done.refs_1_, ...), custom_call_target="tpu_custom_call" | custom-call | flops 2147483648 | bytes 8388608 | tf_op jit(solution)/shard_map/pallas_call | solution.py:325
  118.3 3.7 %collective-permute-done.12.refs_10_ = bf16[1024,128]{1,0:T(8,128)(2,1)S(1)} collective-permute-done((bf16[1024,128]{1,0:T(8,128)(2,1)S(1)}, bf16[1024,128]{1,0:T(8,128)(2,1)S(1)}, u32[]{:S(2)}, u32[]{:S(2)}) %collective-permute-start.12) | collective-permute-done | bytes 262176 | tf_op jit(solution)/shard_map/ppermute | solution.py:248
  122.5 10.7 %collective-permute-done.37.refs_2_ = bf16[512,512]{1,0:T(8,128)(2,1)S(1)} collective-permute-done((bf16[512,512]{1,0:T(8,128)(2,1)S(1)}, bf16[512,512]{1,0:T(8,128)(2,1)S(1)}, u32[]{:S(2)}, u32[]{:S(2)}) %collective-permute-start.37) | collective-permute-done | bytes 524320 | tf_op jit(solution)/shard_map/ppermute | solution.py:248
  133.3 5.6 %collective-permute-done.17.refs_14_ = bf16[1024,128]{1,0:T(8,128)(2,1)S(1)} collective-permute-done((bf16[1024,128]{1,0:T(8,128)(2,1)S(1)}, bf16[1024,128]{1,0:T(8,128)(2,1)S(1)}, u32[]{:S(2)}, u32[]{:S(2)}) %collective-permute-start.17) | collective-permute-done | bytes 262176 | tf_op jit(solution)/shard_map/ppermute | solution.py:248
  140.5 9.0 %collective-permute-done.51.refs_14_ = bf16[512,512]{1,0:T(8,128)(2,1)S(1)} collective-permute-done((bf16[512,512]{1,0:T(8,128)(2,1)S(1)}, bf16[512,512]{1,0:T(8,128)(2,1)S(1)}, u32[]{:S(2)}, u32[]{:S(2)}) %collective-permute-start.51) | collective-permute-done | bytes 524320 | tf_op jit(solution)/shard_map/ppermute | solution.py:248
  150.1 3.1 %shard_map.91.q_ref = bf16[512,256]{1,0:T(8,128)(2,1)S(1)} custom-call(s32[4]{0:T(128)S(1)} %copy-done.20, f32[512,64]{1,0:T(8,128)S(1)} %get-tuple-element.30.cos_ref, f32[512,64]{1,0:T(8,128)S(1)} %get-tuple-element.29.sin_ref, bf16[64,4096]{1,0:T(8,128)(2,1)S(1)} %copy-done, bf16[64,4096]{1,0:T(8,128)(2,1)S(1)} %collective-permute-done.refs_1_, ...), custom_call_target="tpu_custom_call" | custom-call | flops 1073741824 | bytes 6291456 | tf_op jit(solution)/shard_map/pallas_call | solution.py:325
  153.9 3.8 %attend.1 = (bf16[256,256]{1,0:T(8,128)(2,1)S(1)}, bf16[256,256]{1,0:T(8,128)(2,1)S(1)}) custom-call(s32[4]{0:T(128)S(1)} %copy-done.20, bf16[512,256]{1,0:T(8,128)(2,1)S(1)} %shard_map.91.q_ref, f32[2]{0:T(128)S(1)} %copy-done.22, f32[2]{0:T(128)S(1)} %collective-permute-done.19.lam_other, f32[1,256]{1,0:T(1,128)S(1)} %bitcast.21, ...), custom_call_target="tpu_custom_call" | custom-call | flops 1610612736 | bytes 2097152 | tf_op jit(solution)/shard_map/attend/pallas_call | solution.py:361
  158.6 2.6 %collective-permute-start.40 = (bf16[256,256]{1,0:T(8,128)(2,1)S(1)}, bf16[256,256]{1,0:T(8,128)(2,1)S(1)}, u32[]{:S(2)}, u32[]{:S(2)}) collective-permute-start(bf16[256,256]{1,0:T(8,128)(2,1)S(1)} %get-tuple-element.15.refs_0_), channel_id=1, source_target_pairs={{0,16},{1,17},{2,18},{3,19},{4,20},{5,21},{6,22},{7,23},{8,24},{9,... | collective-permute-start | bytes 393224 | tf_op jit(solution)/shard_map/ppermute | solution.py:248
  162.0 1.8 collective-permute-start.41
  166.9 3.5 %collective-permute-start.44 = (bf16[256,256]{1,0:T(8,128)(2,1)S(1)}, bf16[256,256]{1,0:T(8,128)(2,1)S(1)}, u32[]{:S(2)}, u32[]{:S(2)}) collective-permute-start(bf16[256,256]{1,0:T(8,128)(2,1)S(1)} %get-tuple-element.16), channel_id=1, source_target_pairs={{0,18},{1,19},{2,16},{3,17},{4,22},{5,23},{6,20},{7,21},{8,26},{9,... | collective-permute-start | bytes 393224 | tf_op jit(solution)/shard_map/ppermute | solution.py:248
  171.6 3.5 %collective-permute-start.45 = (bf16[256,256]{1,0:T(8,128)(2,1)S(1)}, bf16[256,256]{1,0:T(8,128)(2,1)S(1)}, u32[]{:S(2)}, u32[]{:S(2)}) collective-permute-start(bf16[256,256]{1,0:T(8,128)(2,1)S(1)} %get-tuple-element.16), channel_id=1, source_target_pairs={{0,26},{1,27},{2,24},{3,25},{4,30},{5,31},{6,28},{7,29},{8,18},{9,... | collective-permute-start | bytes 393224 | tf_op jit(solution)/shard_map/ppermute | solution.py:248
  175.1 8.5 %collective-permute-done.44.refs_6_ = bf16[256,256]{1,0:T(8,128)(2,1)S(1)} collective-permute-done((bf16[256,256]{1,0:T(8,128)(2,1)S(1)}, bf16[256,256]{1,0:T(8,128)(2,1)S(1)}, u32[]{:S(2)}, u32[]{:S(2)}) %collective-permute-start.44) | collective-permute-done | bytes 131104 | tf_op jit(solution)/shard_map/ppermute | solution.py:248
  187.9 1.8 out_project.1
  189.8 2.5 %collective-permute-start.53 = (bf16[64,1024]{1,0:T(8,128)(2,1)S(1)}, bf16[64,1024]{1,0:T(8,128)(2,1)S(1)}, u32[]{:S(2)}, u32[]{:S(2)}) collective-permute-start(bf16[64,1024]{1,0:T(8,128)(2,1)S(1)} %get-tuple-element.23), channel_id=1, source_target_pairs={{0,8},{1,9},{2,10},{3,11},{4,12},{5,13},{6,14},{7,15},{8,0},{9,1},... | collective-permute-start | bytes 393224 | tf_op jit(solution)/shard_map/ppermute | solution.py:248
  193.0 1.8 collective-permute-start.55
  196.3 8.1 %collective-permute-done.54 = bf16[64,1024]{1,0:T(8,128)(2,1)S(1)} collective-permute-done((bf16[64,1024]{1,0:T(8,128)(2,1)S(1)}, bf16[64,1024]{1,0:T(8,128)(2,1)S(1)}, u32[]{:S(2)}, u32[]{:S(2)}) %collective-permute-start.54) | collective-permute-done | bytes 131104 | tf_op jit(solution)/shard_map/ppermute | solution.py:248
  (157 shorter events, 47.4 us)
Async XLA Ops:
  3.9 15.2 %collective-permute-start.1 = (bf16[64,4096]{1,0:T(8,128)(2,1)S(1)}, bf16[64,4096]{1,0:T(8,128)(2,1)S(1)}, u32[]{:S(2)}, u32[]{:S(2)}) collective-permute-start(bf16[64,4096]{1,0:T(8,128)(2,1)S(1)} %copy-done), channel_id=1, source_target_pairs={{0,8},{1,9},{2,10},{3,11},{4,12},{5,13},{6,14},{7,15},{8,0},{9,1},... | collective-permute-start | bytes 1572872 | tf_op jit(solution)/shard_map/ppermute | solution.py:248
  6.6 14.0 %collective-permute-start.4 = (bf16[64,4096]{1,0:T(8,128)(2,1)S(1)}, bf16[64,4096]{1,0:T(8,128)(2,1)S(1)}, u32[]{:S(2)}, u32[]{:S(2)}) collective-permute-start(bf16[64,4096]{1,0:T(8,128)(2,1)S(1)} %copy-done), channel_id=1, source_target_pairs={{8,16},{9,17},{10,18},{11,19},{12,20},{13,21},{14,22},{15,23},{16,... | collective-permute-start | bytes 1572872 | tf_op jit(solution)/shard_map/ppermute | solution.py:248
  7.3 34.2 %collective-permute-start = (bf16[64,4096]{1,0:T(8,128)(2,1)S(1)}, bf16[64,4096]{1,0:T(8,128)(2,1)S(1)}, u32[]{:S(2)}, u32[]{:S(2)}) collective-permute-start(bf16[64,4096]{1,0:T(8,128)(2,1)S(1)} %copy-done), channel_id=1, source_target_pairs={{0,2},{1,3},{2,0},{3,1},{4,6},{5,7},{6,4},{7,5},{8,10},{9,11},{10,... | collective-permute-start | bytes 1572872 | tf_op jit(solution)/shard_map/ppermute | solution.py:248
  10.8 30.6 %collective-permute-start.21 = (bf16[512,256]{1,0:T(8,128)(2,1)S(1)}, bf16[512,256]{1,0:T(8,128)(2,1)S(1)}, u32[]{:S(2)}, u32[]{:S(2)}) collective-permute-start(bf16[512,256]{1,0:T(8,128)(2,1)S(1)} %get-tuple-element.20.refs_8_), channel_id=1, source_target_pairs={{0,1},{1,0},{2,3},{3,2},{4,5},{5,4},{6,7},{7,6},{8,9},{9,8},{10,11... | collective-permute-start | bytes 786440 | tf_op jit(solution)/shard_map/ppermute | solution.py:248
  19.1 44.8 %collective-permute-start.3 = (bf16[64,4096]{1,0:T(8,128)(2,1)S(1)}, bf16[64,4096]{1,0:T(8,128)(2,1)}, u32[]{:S(2)}, u32[]{:S(2)}) collective-permute-start(bf16[64,4096]{1,0:T(8,128)(2,1)S(1)} %collective-permute-done.1.refs_2_), channel_id=1, source_target_pairs={{8,16},{9,17},{10,18},{11,19},{12,20},{13,21},{14,22},{15,23},{16,... | collective-permute-start | bytes 1572872 | tf_op jit(solution)/shard_map/ppermute | solution.py:248
  20.6 43.8 %collective-permute-start.5 = (bf16[64,4096]{1,0:T(8,128)(2,1)S(1)}, bf16[64,4096]{1,0:T(8,128)(2,1)}, u32[]{:S(2)}, u32[]{:S(2)}) collective-permute-start(bf16[64,4096]{1,0:T(8,128)(2,1)S(1)} %collective-permute-done.4), channel_id=1, source_target_pairs={{8,0},{9,1},{10,2},{11,3},{12,4},{13,5},{14,6},{15,7},{16,24},{17,... | collective-permute-start | bytes 1572872 | tf_op jit(solution)/shard_map/ppermute | solution.py:248
  22.6 17.3 %collective-permute-start.10 = (bf16[512,128]{1,0:T(8,128)(2,1)S(1)}, bf16[512,128]{1,0:T(8,128)(2,1)}, u32[]{:S(2)}, u32[]{:S(2)}) collective-permute-start(bf16[512,128]{1,0:T(8,128)(2,1)S(1)} %get-tuple-element.27), channel_id=1, source_target_pairs={{0,8},{1,9},{2,10},{3,11},{4,12},{5,13},{6,14},{7,15},{8,0},{9,1},... | collective-permute-start | bytes 393224 | tf_op jit(solution)/shard_map/ppermute | solution.py:248
  42.2 21.7 %collective-permute-start.28 = (bf16[512,256]{1,0:T(8,128)(2,1)}, bf16[512,256]{1,0:T(8,128)(2,1)S(1)}, u32[]{:S(2)}, u32[]{:S(2)}) collective-permute-start(bf16[512,256]{1,0:T(8,128)(2,1)} %get-tuple-element.18), channel_id=1, source_target_pairs={{0,16},{1,17},{2,18},{3,19},{4,20},{5,21},{6,22},{7,23},{8,24},{9,... | collective-permute-start | bytes 786440 | tf_op jit(solution)/shard_map/ppermute | solution.py:248
  46.9 20.1 %collective-permute-start.32 = (bf16[512,256]{1,0:T(8,128)(2,1)S(1)}, bf16[512,256]{1,0:T(8,128)(2,1)S(1)}, u32[]{:S(2)}, u32[]{:S(2)}) collective-permute-start(bf16[512,256]{1,0:T(8,128)(2,1)S(1)} %copy-done.24), channel_id=1, source_target_pairs={{0,24},{1,25},{2,26},{3,27},{4,28},{5,29},{6,30},{7,31},{8,16},{9,... | collective-permute-start | bytes 786440 | tf_op jit(solution)/shard_map/ppermute | solution.py:248
  52.3 15.3 %collective-permute-start.2 = (bf16[64,4096]{1,0:T(8,128)(2,1)S(1)}, bf16[64,4096]{1,0:T(8,128)(2,1)S(1)}, u32[]{:S(2)}, u32[]{:S(2)}) collective-permute-start(bf16[64,4096]{1,0:T(8,128)(2,1)S(1)} %collective-permute-done.1.refs_2_), channel_id=1, source_target_pairs={{0,2},{1,3},{2,0},{3,1},{4,6},{5,7},{6,4},{7,5},{8,10},{9,11},{10,... | collective-permute-start | bytes 1572872 | tf_op jit(solution)/shard_map/ppermute | solution.py:248
  64.4 16.0 %collective-permute-start.7 = (bf16[64,4096]{1,0:T(8,128)(2,1)}, bf16[64,4096]{1,0:T(8,128)(2,1)S(1)}, u32[]{:S(2)}, u32[]{:S(2)}) collective-permute-start(bf16[64,4096]{1,0:T(8,128)(2,1)} %collective-permute-done.3), channel_id=1, source_target_pairs={{8,0},{9,1},{10,2},{11,3},{12,4},{13,5},{14,6},{15,7},{16,24},{17,... | collective-permute-start | bytes 1572872 | tf_op jit(solution)/shard_map/ppermute | solution.py:248
  67.0 14.0 %collective-permute-start.26 = (bf16[512,256]{1,0:T(8,128)(2,1)S(1)}, bf16[512,256]{1,0:T(8,128)(2,1)S(1)}, u32[]{:S(2)}, u32[]{:S(2)}) collective-permute-start(bf16[512,256]{1,0:T(8,128)(2,1)S(1)} %collective-permute-done.24.refs_12_), channel_id=1, source_target_pairs={{0,4},{1,5},{2,6},{3,7},{4,0},{5,1},{6,2},{7,3},{8,12},{9,13},{10,... | collective-permute-start | bytes 786440 | tf_op jit(solution)/shard_map/ppermute | solution.py:248
  67.6 15.0 %collective-permute-start.29 = (bf16[512,256]{1,0:T(8,128)(2,1)S(1)}, bf16[512,256]{1,0:T(8,128)(2,1)S(1)}, u32[]{:S(2)}, u32[]{:S(2)}) collective-permute-start(bf16[512,256]{1,0:T(8,128)(2,1)S(1)} %collective-permute-done.28.refs_16_), channel_id=1, source_target_pairs={{0,1},{1,0},{2,3},{3,2},{4,5},{5,4},{6,7},{7,6},{8,9},{9,8},{10,11... | collective-permute-start | bytes 786440 | tf_op jit(solution)/shard_map/ppermute | solution.py:248
  67.6 15.5 %collective-permute-start.30 = (bf16[512,256]{1,0:T(8,128)(2,1)S(1)}, bf16[512,256]{1,0:T(8,128)(2,1)S(1)}, u32[]{:S(2)}, u32[]{:S(2)}) collective-permute-start(bf16[512,256]{1,0:T(8,128)(2,1)S(1)} %collective-permute-done.28.refs_16_), channel_id=1, source_target_pairs={{0,4},{1,5},{2,6},{3,7},{4,0},{5,1},{6,2},{7,3},{8,12},{9,13},{10,... | collective-permute-start | bytes 786440 | tf_op jit(solution)/shard_map/ppermute | solution.py:248
  69.2 14.0 %collective-permute-start.33 = (bf16[512,256]{1,0:T(8,128)(2,1)S(1)}, bf16[512,256]{1,0:T(8,128)(2,1)S(1)}, u32[]{:S(2)}, u32[]{:S(2)}) collective-permute-start(bf16[512,256]{1,0:T(8,128)(2,1)S(1)} %collective-permute-done.32.refs_20_), channel_id=1, source_target_pairs={{0,1},{1,0},{2,3},{3,2},{4,5},{5,4},{6,7},{7,6},{8,9},{9,8},{10,11... | collective-permute-start | bytes 786440 | tf_op jit(solution)/shard_map/ppermute | solution.py:248
  81.0 14.9 %collective-permute-start.6 = (bf16[64,4096]{1,0:T(8,128)(2,1)S(1)}, bf16[64,4096]{1,0:T(8,128)(2,1)S(1)}, u32[]{:S(2)}, u32[]{:S(2)}) collective-permute-start(bf16[64,4096]{1,0:T(8,128)(2,1)S(1)} %broadcast_select_fusion.1.refs_4_), channel_id=1, source_target_pairs={{0,2},{1,3},{2,0},{3,1},{4,6},{5,7},{6,4},{7,5},{8,10},{9,11},{10,... | collective-permute-start | bytes 1572872 | tf_op jit(solution)/shard_map/ppermute | solution.py:248
  82.6 24.5 %collective-permute-start.8 = (bf16[64,4096]{1,0:T(8,128)(2,1)S(1)}, bf16[64,4096]{1,0:T(8,128)(2,1)S(1)}, u32[]{:S(2)}, u32[]{:S(2)}) collective-permute-start(bf16[64,4096]{1,0:T(8,128)(2,1)S(1)} %broadcast_select_fusion.refs_6_), channel_id=1, source_target_pairs={{0,2},{1,3},{2,0},{3,1},{4,6},{5,7},{6,4},{7,5},{8,10},{9,11},{10,... | collective-permute-start | bytes 1572872 | tf_op jit(solution)/shard_map/ppermute | solution.py:248
  88.8 26.6 %collective-permute-start.47 = (bf16[512,512]{1,0:T(8,128)(2,1)S(1)}, bf16[512,512]{1,0:T(8,128)(2,1)S(1)}, u32[]{:S(2)}, u32[]{:S(2)}) collective-permute-start(bf16[512,512]{1,0:T(8,128)(2,1)S(1)} %copy-done.1), channel_id=1, source_target_pairs={{0,4},{1,5},{2,6},{3,7},{4,0},{5,1},{6,2},{7,3},{8,12},{9,13},{10,... | collective-permute-start | bytes 1572872 | tf_op jit(solution)/shard_map/ppermute | solution.py:248
  90.4 25.9 %collective-permute-start.49 = (bf16[512,512]{1,0:T(8,128)(2,1)S(1)}, bf16[512,512]{1,0:T(8,128)(2,1)S(1)}, u32[]{:S(2)}, u32[]{:S(2)}) collective-permute-start(bf16[512,512]{1,0:T(8,128)(2,1)S(1)} %copy-done.1), channel_id=1, source_target_pairs={{0,2},{1,3},{2,0},{3,1},{4,6},{5,7},{6,4},{7,5},{8,10},{9,11},{10,... | collective-permute-start | bytes 1572872 | tf_op jit(solution)/shard_map/ppermute | solution.py:248
  92.0 20.7 %collective-permute-start.19 = (f32[2]{0:T(128)S(1)}, f32[2]{0:T(128)S(1)}, u32[]{:S(2)}, u32[]{:S(2)}) collective-permute-start(f32[2]{0:T(128)S(1)} %copy-done.22), channel_id=1, source_target_pairs={{0,1},{1,0},{2,3},{3,2},{4,5},{5,4},{6,7},{7,6},{8,9},{9,8},{10,11... | collective-permute-start | bytes 32 | tf_op jit(solution)/shard_map/ppermute | solution.py:248
  95.9 16.9 %collective-permute-start.14 = (bf16[512,128]{1,0:T(8,128)(2,1)S(1)}, bf16[512,128]{1,0:T(8,128)(2,1)S(1)}, u32[]{:S(2)}, u32[]{:S(2)}) collective-permute-start(bf16[512,128]{1,0:T(8,128)(2,1)S(1)} %copy-done.27), channel_id=1, source_target_pairs={{0,16},{1,17},{2,18},{3,19},{4,20},{5,21},{6,22},{7,23},{8,24},{9,... | collective-permute-start | bytes 393224 | tf_op jit(solution)/shard_map/ppermute | solution.py:248
  114.4 18.9 %collective-permute-start.37 = (bf16[512,512]{1,0:T(8,128)(2,1)S(1)}, bf16[512,512]{1,0:T(8,128)(2,1)S(1)}, u32[]{:S(2)}, u32[]{:S(2)}) collective-permute-start(bf16[512,512]{1,0:T(8,128)(2,1)S(1)} %shard_map.92.refs_0_), channel_id=1, source_target_pairs={{0,4},{1,5},{2,6},{3,7},{4,0},{5,1},{6,2},{7,3},{8,12},{9,13},{10,... | collective-permute-start | bytes 1572872 | tf_op jit(solution)/shard_map/ppermute | solution.py:248
  116.3 22.6 %collective-permute-start.17 = (bf16[1024,128]{1,0:T(8,128)(2,1)S(1)}, bf16[1024,128]{1,0:T(8,128)(2,1)S(1)}, u32[]{:S(2)}, u32[]{:S(2)}) collective-permute-start(bf16[1024,128]{1,0:T(8,128)(2,1)S(1)} %constant_dynamic-update-slice_fusion.refs_12_), channel_id=1, source_target_pairs={{0,4},{1,5},{2,6},{3,7},{4,0},{5,1},{6,2},{7,3},{8,12},{9,13},{10,... | collective-permute-start | bytes 786440 | tf_op jit(solution)/shard_map/ppermute | solution.py:248
  117.8 31.7 %collective-permute-start.51 = (bf16[512,512]{1,0:T(8,128)(2,1)S(1)}, bf16[512,512]{1,0:T(8,128)(2,1)S(1)}, u32[]{:S(2)}, u32[]{:S(2)}) collective-permute-start(bf16[512,512]{1,0:T(8,128)(2,1)S(1)} %collective-permute-done.49.refs_12_), channel_id=1, source_target_pairs={{0,4},{1,5},{2,6},{3,7},{4,0},{5,1},{6,2},{7,3},{8,12},{9,13},{10,... | collective-permute-start | bytes 1572872 | tf_op jit(solution)/shard_map/ppermute | solution.py:248
  122.0 27.6 %collective-permute-start.36 = (bf16[512,512]{1,0:T(8,128)(2,1)S(1)}, bf16[512,512]{1,0:T(8,128)(2,1)S(1)}, u32[]{:S(2)}, u32[]{:S(2)}) collective-permute-start(bf16[512,512]{1,0:T(8,128)(2,1)S(1)} %shard_map.92.refs_0_), channel_id=1, source_target_pairs={{0,1},{1,0},{2,3},{3,2},{4,5},{5,4},{6,7},{7,6},{8,9},{9,8},{10,11... | collective-permute-start | bytes 1572872 | tf_op jit(solution)/shard_map/ppermute | solution.py:248
  122.0 16.9 %collective-permute-start.13 = (bf16[1024,128]{1,0:T(8,128)(2,1)S(1)}, bf16[1024,128]{1,0:T(8,128)(2,1)S(1)}, u32[]{:S(2)}, u32[]{:S(2)}) collective-permute-start(bf16[1024,128]{1,0:T(8,128)(2,1)S(1)} %collective-permute-done.12.refs_10_), channel_id=1, source_target_pairs={{0,1},{1,0},{2,3},{3,2},{4,5},{5,4},{6,7},{7,6},{8,9},{9,8},{10,11... | collective-permute-start | bytes 786440 | tf_op jit(solution)/shard_map/ppermute | solution.py:248
  133.3 19.9 %collective-permute-start.38 = (bf16[512,512]{1,0:T(8,128)(2,1)S(1)}, bf16[512,512]{1,0:T(8,128)(2,1)S(1)}, u32[]{:S(2)}, u32[]{:S(2)}) collective-permute-start(bf16[512,512]{1,0:T(8,128)(2,1)S(1)} %collective-permute-done.37.refs_2_), channel_id=1, source_target_pairs={{0,1},{1,0},{2,3},{3,2},{4,5},{5,4},{6,7},{7,6},{8,9},{9,8},{10,11... | collective-permute-start | bytes 1572872 | tf_op jit(solution)/shard_map/ppermute | solution.py:248
  138.9 18.9 %collective-permute-start.46 = (bf16[512,512]{1,0:T(8,128)(2,1)S(1)}, bf16[512,512]{1,0:T(8,128)(2,1)S(1)}, u32[]{:S(2)}, u32[]{:S(2)}) collective-permute-start(bf16[512,512]{1,0:T(8,128)(2,1)S(1)} %copy-done.1), channel_id=1, source_target_pairs={{0,1},{1,0},{2,3},{3,2},{4,5},{5,4},{6,7},{7,6},{8,9},{9,8},{10,11... | collective-permute-start | bytes 1572872 | tf_op jit(solution)/shard_map/ppermute | solution.py:248
  140.4 20.8 %collective-permute-start.48 = (bf16[512,512]{1,0:T(8,128)(2,1)S(1)}, bf16[512,512]{1,0:T(8,128)(2,1)S(1)}, u32[]{:S(2)}, u32[]{:S(2)}) collective-permute-start(bf16[512,512]{1,0:T(8,128)(2,1)S(1)} %collective-permute-done.47.refs_10_), channel_id=1, source_target_pairs={{0,1},{1,0},{2,3},{3,2},{4,5},{5,4},{6,7},{7,6},{8,9},{9,8},{10,11... | collective-permute-start | bytes 1572872 | tf_op jit(solution)/shard_map/ppermute | solution.py:248
  149.6 14.2 %collective-permute-start.50 = (bf16[512,512]{1,0:T(8,128)(2,1)S(1)}, bf16[512,512]{1,0:T(8,128)(2,1)S(1)}, u32[]{:S(2)}, u32[]{:S(2)}) collective-permute-start(bf16[512,512]{1,0:T(8,128)(2,1)S(1)} %collective-permute-done.49.refs_12_), channel_id=1, source_target_pairs={{0,1},{1,0},{2,3},{3,2},{4,5},{5,4},{6,7},{7,6},{8,9},{9,8},{10,11... | collective-permute-start | bytes 1572872 | tf_op jit(solution)/shard_map/ppermute | solution.py:248
  149.6 16.5 %collective-permute-start.52 = (bf16[512,512]{1,0:T(8,128)(2,1)S(1)}, bf16[512,512]{1,0:T(8,128)(2,1)S(1)}, u32[]{:S(2)}, u32[]{:S(2)}) collective-permute-start(bf16[512,512]{1,0:T(8,128)(2,1)S(1)} %collective-permute-done.51.refs_14_), channel_id=1, source_target_pairs={{0,1},{1,0},{2,3},{3,2},{4,5},{5,4},{6,7},{7,6},{8,9},{9,8},{10,11... | collective-permute-start | bytes 1572872 | tf_op jit(solution)/shard_map/ppermute | solution.py:248
  166.9 16.8 %collective-permute-start.44 = (bf16[256,256]{1,0:T(8,128)(2,1)S(1)}, bf16[256,256]{1,0:T(8,128)(2,1)S(1)}, u32[]{:S(2)}, u32[]{:S(2)}) collective-permute-start(bf16[256,256]{1,0:T(8,128)(2,1)S(1)} %get-tuple-element.16), channel_id=1, source_target_pairs={{0,18},{1,19},{2,16},{3,17},{4,22},{5,23},{6,20},{7,21},{8,26},{9,... | collective-permute-start | bytes 393224 | tf_op jit(solution)/shard_map/ppermute | solution.py:248
  (52 other events, 467.3 us)
